TPU v7x, 32 devices: a whole 2x2x4 slice. The times are simulated.
32 devices in a mesh: sp: 8 (over z, x), tp: 4 (over y, core).
Axes of the slice: x: 2, y: 2, z: 4, core: 2. Of those that a mesh axis runs over, the one named last changes fastest.
Arguments:
- latent: bfloat16 [4096, 4096], P('sp'), may hold values from -64 to 64
- context: bfloat16 [512, 4096], P('sp'), may hold values from -6 to 6
- condition: bfloat16 [4096], P('sp'), may hold values from -6 to 6
- context_condition: bfloat16 [4096], P('sp'), may hold values from -6 to 6
- shift_weight: bfloat16 [4096, 4096], P('sp', 'tp'), may hold values from -0.125 to 0.125
- scale_weight: bfloat16 [4096, 4096], P('sp', 'tp'), may hold values from -0.125 to 0.125
- gate_weight: bfloat16 [4096, 4096], P('sp', 'tp'), may hold values from -0.25 to 0.25
- norm_gain: float32 [4096], replicated, may hold values from 0.1 to 1.9
- query_weight: bfloat16 [4096, 2048], P(None, 'tp'), may hold values from -0.09375 to 0.09375
- key_weight: bfloat16 [4096, 2048], P(None, 'tp'), may hold values from -0.09375 to 0.09375
- value_weight: bfloat16 [4096, 2048], P(None, 'tp'), may hold values from -0.09375 to 0.09375
- write_weight: bfloat16 [4096, 2, 16], replicated, may hold values from -0.09375 to 0.09375
- decay_weight: bfloat16 [4096, 2, 16], replicated, may hold values from -0.09375 to 0.09375
- write_bias: float32 [2, 16], replicated, may hold values from -12 to 1
- decay_bias: float32 [2, 16], replicated, may hold values from -16 to -4
- log_rate: float32 [2, 16], replicated, may hold values from 0 to 1.4
- head_gain: float32 [128], replicated, may hold values from 0.1 to 1.9
- out_weight: bfloat16 [2048, 4096], P(None, 'tp'), may hold values from -0.125 to 0.125
Outputs:
- updated: bfloat16 [4096, 4096], P('sp', 'tp')
All inputs are finite; a program needn't handle non-finite values.
Results may differ from a plain program's by a relative error of at most 0.013.
Values may be sent and summed in bfloat16 or wider, within the bound.
A program may use at most 128 MiB of HBM per device.

v0:
```python
import functools

import jax
import jax.numpy as jnp
from jax import lax
from jax.experimental import pallas as pl
from jax.experimental.pallas import tpu as pltpu
from jax.sharding import PartitionSpec as P

HEAD_DIM = 128
CHUNK = 128
epsilon = 0.0001
bf16 = jnp.bfloat16
f32 = jnp.float32


def mm(a, b):
    return jnp.dot(a.astype(bf16), b.astype(bf16), preferred_element_type=f32)


def spans(tokens, ctx_tokens):
    size = min(CHUNK, tokens)
    lat = [(at, size) for at in range(0, tokens, size)]
    ctx_size = min(CHUNK, ctx_tokens)
    ctx = [(tokens + at, ctx_size) for at in range(0, ctx_tokens, ctx_size)]
    return lat, ctx


def prep_kernel(tokens, ctx_tokens, q_ref, k_ref, v_ref, col_ref, row_ref, o_ref, e_ref, map_ref):
    lat, ctx = spans(tokens, ctx_tokens)
    items = []
    shared = {}
    for at, size in lat + ctx:
        keys = k_ref[at : at + size, :]
        keys_t = keys.astype(f32).T
        gram = jnp.dot(keys, keys_t.astype(bf16), preferred_element_type=f32)
        rows = lax.broadcasted_iota(jnp.int32, (size, size), 0)
        cols = lax.broadcasted_iota(jnp.int32, (size, size), 1)
        diag = jnp.where(rows == cols, gram, 0.0)
        s_col = lax.rsqrt(jnp.sum(diag, axis=1, keepdims=True) + epsilon)
        s_row = lax.rsqrt(jnp.sum(diag, axis=0, keepdims=True) + epsilon)
        gram = gram * s_col * s_row
        entry = dict(keys=keys.astype(f32) * s_col, keys_t=keys_t * s_row, values=v_ref[at : at + size, :].astype(f32))
        if at < tokens:
            queries = q_ref[at : at + size, :].astype(f32)
            q_scale = lax.rsqrt(jnp.sum(queries * queries, axis=1, keepdims=True) + epsilon) * HEAD_DIM**-0.5
            entry["queries"] = queries * q_scale
            entry["score"] = (
                jnp.dot(q_ref[at : at + size, :], keys_t.astype(bf16), preferred_element_type=f32) * q_scale * s_row
            )
        shared[at] = entry
        for d in range(2):
            rate_col = col_ref[0, at : at + size, 2 * d : 2 * d + 1]
            run_col = col_ref[0, at : at + size, 2 * d + 1 : 2 * d + 2]
            run_row = row_ref[0, 2 * d + 1 : 2 * d + 2, at : at + size]
            inside = rows >= cols if d == 0 else rows <= cols
            strict = rows > cols if d == 0 else rows < cols
            decay = jnp.where(inside, jnp.exp(jnp.minimum(run_col - run_row, 0.0)), 0.0)
            system = jnp.where(strict, gram * decay * rate_col, 0.0)
            item = dict(at=at, size=size, d=d, rate_col=rate_col, run_col=run_col, run_row=run_row)
            item["system"] = system
            if at < tokens:
                item["score"] = entry["score"] * decay
            near = (rows // 2) == (cols // 2)
            item["inv"] = jnp.where(rows == cols, 1.0, jnp.where(near, -system, 0.0))
            items.append(item)
    span = 2
    while span < max(item["size"] for item in items):
        firsts = []
        for item in items:
            if span >= item["size"]:
                firsts.append(None)
                continue
            size = item["size"]
            rows = lax.broadcasted_iota(jnp.int32, (size, size), 0) // span
            cols = lax.broadcasted_iota(jnp.int32, (size, size), 1) // span
            if item["d"] == 0:
                mask = ((rows % 2) == 1) & (cols == rows - 1)
            else:
                mask = ((cols % 2) == 1) & (rows == cols - 1)
            firsts.append(mm(jnp.where(mask, item["system"], 0.0), item["inv"]))
        for item, first in zip(items, firsts):
            if first is not None:
                item["inv"] = item["inv"] - mm(item["inv"], first)
        span *= 2
    for item in items:
        entry = shared[item["at"]]
        growth = jnp.exp(item["run_col"])
        both = jnp.concatenate(
            [entry["values"] * item["rate_col"], entry["keys"] * (item["rate_col"] * growth)], axis=1
        )
        item["solved"] = mm(item["inv"], both)
        last = item["run_row"][:, item["size"] - 1 :] if item["d"] == 0 else item["run_row"][:, :1]
        item["gate"] = jnp.exp(last)
        late_t = entry["keys_t"] * jnp.exp(last - item["run_row"])
        item["late"] = mm(late_t, item["solved"])
        if item["at"] < tokens:
            weighed = mm(item["score"], item["solved"])
            item["local"] = weighed[:, :HEAD_DIM]
            item["early"] = entry["queries"] * growth - weighed[:, HEAD_DIM:]
    eye_r = lax.broadcasted_iota(jnp.int32, (HEAD_DIM, HEAD_DIM), 0)
    eye_c = lax.broadcasted_iota(jnp.int32, (HEAD_DIM, HEAD_DIM), 1)
    eye = (eye_r == eye_c).astype(f32)

    def chain(chunks, d, emit):
        carry = None
        for item in chunks if d == 0 else chunks[::-1]:
            if emit:
                if carry is None:
                    out, early = item["local"], item["early"]
                else:
                    moved = mm(item["early"], carry)
                    out = item["local"] + moved[:, :HEAD_DIM]
                    early = item["early"] + moved[:, HEAD_DIM:]
                e_ref[0, item["at"] : item["at"] + item["size"], d * HEAD_DIM : (d + 1) * HEAD_DIM] = early.astype(
                    bf16
                )
                item["out"] = out
            late, gate = item["late"], item["gate"]
            fresh = jnp.concatenate([late[:, :HEAD_DIM], (gate - 1.0) * eye - late[:, HEAD_DIM:]], axis=1)
            if carry is None:
                carry = fresh
            else:
                carry = gate * carry + fresh - mm(late[:, HEAD_DIM:], carry)
        return carry

    for d in range(2):
        latents = [i for i in items if i["d"] == d and i["at"] < tokens]
        contexts = [i for i in items if i["d"] == d and i["at"] >= tokens]
        map_ref[0, d] = chain(contexts, d, False).astype(bf16)
        map_ref[1, d] = chain(latents, d, True).astype(bf16)
    for at, size in lat:
        pair = [i for i in items if i["at"] == at]
        o_ref[0, at : at + size, :] = pair[0]["out"] + pair[1]["out"]


def apply_maps(maps, state):
    high = state.astype(bf16)
    low = (state - high.astype(f32)).astype(bf16)
    move = maps[:, HEAD_DIM:]
    return (
        state
        + maps[:, :HEAD_DIM].astype(f32)
        + jnp.dot(move, high, preferred_element_type=f32)
        + jnp.dot(move, low, preferred_element_type=f32)
    )


def on_mesh(sp=None, tp=None):
    return (lax.axis_index("sp") if sp is None else sp, lax.axis_index("tp") if tp is None else tp)


def send(src, dst, send_sem, recv_sem, device):
    return pltpu.make_async_remote_copy(
        src_ref=src,
        dst_ref=dst,
        send_sem=send_sem,
        recv_sem=recv_sem,
        device_id=device,
        device_id_type=pl.DeviceIdType.MESH,
    )


def greet(devices):
    barrier = pltpu.get_barrier_semaphore()
    for device in devices:
        pl.semaphore_signal(barrier, inc=1, device_id=device, device_id_type=pl.DeviceIdType.MESH)


def modulation_kernel(
    sp, tp, silu_ref, shift_ref, scale_ref, gate_ref, rows_ref, gate_out, got, blocks, sent_a, recv_a, sent_b, recv_b
):
    me, col = lax.axis_index("sp"), lax.axis_index("tp")
    width = shift_ref.shape[1]
    rings = [on_mesh(sp=lax.rem(me + r, sp)) for r in range(1, sp)]
    cross = [on_mesh(tp=lax.rem(col + r, tp)) for r in range(1, tp)]
    greet(rings + cross)
    silu = silu_ref[...]
    shift = jnp.dot(silu, shift_ref[...], preferred_element_type=f32)
    scale = jnp.dot(silu, scale_ref[...], preferred_element_type=f32)
    gate = jnp.dot(silu, gate_ref[...], preferred_element_type=f32)
    got[me] = jnp.concatenate([shift[0:2], scale[0:2], gate[0:1], jnp.zeros((3, width), f32)], axis=0)
    pl.semaphore_wait(pltpu.get_barrier_semaphore(), len(rings) + len(cross))
    out = []
    for r, device in enumerate(rings):
        out.append(send(got.at[me], got.at[me], sent_a.at[r], recv_a.at[me], device))
        out[-1].start()
    for r in range(1, sp):
        src = lax.rem(me + r, sp)
        send(got.at[src], got.at[src], sent_a.at[0], recv_a.at[src], on_mesh(sp=src)).wait_recv()
    total = got[0]
    for place in range(1, sp):
        total = total + got[place]
    blocks[col] = total
    gate_out[...] = total[4:5]
    for r, device in enumerate(cross):
        out.append(send(blocks.at[col], blocks.at[col], sent_b.at[r], recv_b.at[col], device))
        out[-1].start()
    for r in range(1, tp):
        src = lax.rem(col + r, tp)
        send(blocks.at[src], blocks.at[src], sent_b.at[0], recv_b.at[src], on_mesh(tp=src)).wait_recv()
    for place in range(tp):
        rows_ref[:, place * width : (place + 1) * width] = blocks[place][0:4]
    for copy in out:
        copy.wait_send()


def modulation(silu_rows, shift_weight, scale_weight, gate_weight):
    sp, tp = lax.axis_size("sp"), lax.axis_size("tp")
    width = shift_weight.shape[1]
    vmem = pl.BlockSpec(memory_space=pltpu.VMEM)
    return pl.pallas_call(
        functools.partial(modulation_kernel, sp, tp),
        in_specs=[vmem] * 4,
        out_specs=[vmem] * 2,
        out_shape=[jax.ShapeDtypeStruct((4, tp * width), f32), jax.ShapeDtypeStruct((1, width), f32)],
        scratch_shapes=[
            pltpu.VMEM((sp, 8, width), f32),
            pltpu.VMEM((tp, 8, width), f32),
            pltpu.SemaphoreType.DMA((sp,)),
            pltpu.SemaphoreType.DMA((sp,)),
            pltpu.SemaphoreType.DMA((tp,)),
            pltpu.SemaphoreType.DMA((tp,)),
        ],
        compiler_params=pltpu.CompilerParams(collective_id=0, has_side_effects=True),
        name="modulation",
    )(jnp.pad(silu_rows, ((0, 6), (0, 0))), shift_weight, scale_weight, gate_weight)


def exchange_kernel(
    sp, per, tokens, ctx_tokens, q_ref, k_ref, v_ref, col_ref, row_ref, gain_ref, out_ref,
    o_ref, e_ref, maps_ref, got, starts, back, sent_a, recv_a, sent_b, recv_b,
):
    me = lax.axis_index("sp")
    heads = col_ref.shape[0]
    items = 2 * heads
    peers = [lax.rem(me + r, sp) for r in range(1, sp)]
    greet([on_mesh(sp=peer) for peer in peers])
    pl.semaphore_wait(pltpu.get_barrier_semaphore(), sp - 1)

    def ship(part, item):
        owner, slot = item // per, lax.rem(item, per)
        return owner, send(
            maps_ref.at[part, item],
            got.at[part, me, slot],
            sent_a.at[part, item],
            recv_a.at[part, me, slot],
            on_mesh(sp=owner),
        )

    def one_head(k, unused):
        head = lax.rem(me * per // 2 + heads // 2 + k + (heads - heads // 2 + 1), heads)
        lanes = pl.ds(pl.multiple_of(head * HEAD_DIM, HEAD_DIM), HEAD_DIM)
        prep_kernel(
            tokens,
            ctx_tokens,
            q_ref.at[:, lanes],
            k_ref.at[:, lanes],
            v_ref.at[:, lanes],
            col_ref.at[pl.ds(head, 1)],
            row_ref.at[pl.ds(head, 1)],
            o_ref.at[pl.ds(head, 1)],
            e_ref.at[pl.ds(head, 1)],
            maps_ref.at[:, pl.ds(2 * head, 2)],
        )
        for d in range(2):
            for part in range(2):
                owner, copy = ship(part, 2 * head + d)

                @pl.when(owner != me)
                def _():
                    copy.start()

                @pl.when(owner == me)
                def _():
                    got[part, me, lax.rem(2 * head + d, per)] = maps_ref[part, 2 * head + d]

        return unused

    lax.fori_loop(0, heads, one_head, 0)

    def arrive(part, slot):
        for peer in peers:
            spot = got.at[part, peer, slot]
            send(spot, spot, sent_a.at[part, 0], recv_a.at[part, peer, slot], on_mesh(sp=peer)).wait_recv()

    def give_back(place, slot):
        return send(
            starts.at[place, slot],
            back.at[me, slot],
            sent_b.at[place, slot],
            recv_b.at[me, slot],
            on_mesh(sp=place),
        )

    for slot in range(per):

        @pl.when(me * per + slot < items)
        def _():
            reverse = lax.rem(me * per + slot, 2)
            arrive(0, slot)
            state = jnp.zeros((HEAD_DIM, HEAD_DIM), f32)
            for step in range(sp):
                state = apply_maps(got[0, step + reverse * (sp - 1 - 2 * step), slot], state)
            arrive(1, slot)
            for step in range(sp):
                place = step + reverse * (sp - 1 - 2 * step)
                starts[place, slot] = state.astype(bf16)

                @pl.when(place != me)
                def _():
                    give_back(place, slot).start()

                @pl.when(place == me)
                def _():
                    back[me, slot] = starts[me, slot]

                if step < sp - 1:
                    state = apply_maps(got[1, place, slot], state)

    for item in range(items):
        owner, slot = item // per, item % per

        @pl.when(owner != me)
        def _():
            spot = back.at[owner, slot]
            send(spot, spot, sent_b.at[owner, slot], recv_b.at[owner, slot], on_mesh(sp=owner)).wait_recv()

    for head in range(heads):
        pair = [back[item // per, item % per] for item in (2 * head, 2 * head + 1)]
        combined = o_ref[head] + jnp.dot(
            e_ref[head], jnp.concatenate(pair, axis=0), preferred_element_type=f32
        )
        scale = lax.rsqrt(jnp.mean(combined * combined, axis=1, keepdims=True) + epsilon)
        out_ref[:, head * HEAD_DIM : (head + 1) * HEAD_DIM] = (combined * scale * gain_ref[...]).astype(bf16)
    for item in range(items):
        for part in range(2):
            owner, copy = ship(part, item)

            @pl.when(owner != me)
            def _():
                copy.wait_send()

    for slot in range(per):

        @pl.when(me * per + slot < items)
        def _():
            for peer in peers:
                give_back(peer, slot).wait_send()


def exchange(queries, keys, values, col, row, gain, tokens, ctx_tokens):
    heads = col.shape[0]
    items = 2 * heads
    sp = lax.axis_size("sp")
    per = -(-items // sp)
    vmem = pl.BlockSpec(memory_space=pltpu.VMEM)
    dma = pltpu.SemaphoreType.DMA
    return pl.pallas_call(
        functools.partial(exchange_kernel, sp, per, tokens, ctx_tokens),
        in_specs=[vmem] * 6,
        out_specs=vmem,
        out_shape=jax.ShapeDtypeStruct((tokens, heads * HEAD_DIM), bf16),
        scratch_shapes=[
            pltpu.VMEM((heads, tokens, HEAD_DIM), f32),
            pltpu.VMEM((heads, tokens, 2 * HEAD_DIM), bf16),
            pltpu.VMEM((2, items, HEAD_DIM, 2 * HEAD_DIM), bf16),
            pltpu.VMEM((2, sp, per, HEAD_DIM, 2 * HEAD_DIM), bf16),
            pltpu.VMEM((sp, per, HEAD_DIM, HEAD_DIM), bf16),
            pltpu.VMEM((sp, per, HEAD_DIM, HEAD_DIM), bf16),
            dma((2, items)),
            dma((2, sp, per)),
            dma((sp, per)),
            dma((sp, per)),
        ],
        compiler_params=pltpu.CompilerParams(
            collective_id=1, has_side_effects=True, vmem_limit_bytes=48 * 1024 * 1024
        ),
        name="exchange",
    )(queries, keys, values, col, row, gain)


def output_kernel(
    tp, pieces, head_ref, gate_ref, latent_ref, weight_ref, out_ref,
    got, weight, residual, acc, local_sems, sent_y, recv_y, sent_c, recv_c, sent_r, recv_r,
):
    me, col = lax.axis_index("sp"), lax.axis_index("tp")
    core = lax.rem(col, 2)
    partner = col + 1 - 2 * core
    chips = tp // 2
    far = [lax.rem(col + 2 * r, tp) for r in range(1, chips)]
    far_partner = [place + 1 - 2 * core for place in far]
    tokens, depth = head_ref.shape
    width = out_ref.shape[1]
    rows = tokens // pieces
    load = pltpu.make_async_copy(weight_ref, weight, local_sems.at[0])
    load.start()
    take = pltpu.make_async_copy(
        latent_ref.at[:, pl.ds(pl.multiple_of(col * width, width), width)], residual, local_sems.at[1]
    )
    take.start()
    greet([on_mesh(tp=place) for place in [partner] + far])
    pl.semaphore_wait(pltpu.get_barrier_semaphore(), chips)
    out = []

    def piece(ref, p):
        return ref.at[pl.ds(p * rows, rows)]

    for p in range(pieces):
        for r, place in enumerate(far):
            out.append(
                send(piece(head_ref, p), piece(got.at[col], p), sent_y.at[r, p], recv_y.at[col, p], on_mesh(tp=place))
            )
            out[-1].start()
    for p in range(pieces):
        out.append(
            send(piece(head_ref, p), piece(got.at[col], p), sent_c.at[p], recv_c.at[p], on_mesh(tp=partner))
        )
        out[-1].start()
    load.wait()

    def weights(src):
        return weight[pl.ds(pl.multiple_of(src * depth, depth), depth), :]

    def add(p, block, src, first=False):
        part = jnp.dot(block, weights(src), preferred_element_type=f32)
        at = pl.ds(p * rows, rows)
        acc[at, :] = part if first else acc[at, :] + part

    for p in range(pieces):
        add(p, head_ref[pl.ds(p * rows, rows), :], col, True)
    for p in range(pieces):
        spot = piece(got.at[partner], p)
        send(spot, spot, sent_c.at[p], recv_c.at[p], on_mesh(tp=partner)).wait_recv()
        add(p, spot[...], partner)
    take.wait()
    for p in range(pieces):
        for r, src in enumerate(far):
            spot = piece(got.at[src], p)
            send(spot, spot, sent_y.at[r, p], recv_y.at[src, p], on_mesh(tp=src)).wait_recv()
            out.append(send(spot, spot, sent_r.at[r, p], recv_r.at[src, p], on_mesh(tp=partner)))
            out[-1].start()
            add(p, spot[...], src)
        for r, src in enumerate(far_partner):
            spot = piece(got.at[src], p)
            send(spot, spot, sent_r.at[r, p], recv_r.at[src, p], on_mesh(tp=partner)).wait_recv()
            add(p, spot[...], src)
        at = pl.ds(p * rows, rows)
        out_ref[at, :] = (residual[at, :].astype(f32) + gate_ref[...] * acc[at, :]).astype(bf16)
    for copy in out:
        copy.wait_send()


def output(head_out, gate_row, latent, out_weight):
    tp = lax.axis_size("tp")
    tokens, depth = head_out.shape
    width = out_weight.shape[1]
    pieces = 4
    vmem = pl.BlockSpec(memory_space=pltpu.VMEM)
    anywhere = pl.BlockSpec(memory_space=pl.ANY)
    dma = pltpu.SemaphoreType.DMA
    return pl.pallas_call(
        functools.partial(output_kernel, tp, pieces),
        in_specs=[vmem, vmem, anywhere, anywhere],
        out_specs=vmem,
        out_shape=jax.ShapeDtypeStruct((tokens, width), bf16),
        scratch_shapes=[
            pltpu.VMEM((tp, tokens, depth), bf16),
            pltpu.VMEM(out_weight.shape, bf16),
            pltpu.VMEM((tokens, width), bf16),
            pltpu.VMEM((tokens, width), f32),
            dma((2,)),
            dma((tp, pieces)),
            dma((tp, pieces)),
            dma((pieces,)),
            dma((pieces,)),
            dma((tp, pieces)),
            dma((tp, pieces)),
        ],
        compiler_params=pltpu.CompilerParams(
            collective_id=2, has_side_effects=True, vmem_limit_bytes=63 * 1024 * 1024
        ),
        name="output",
    )(head_out, gate_row, latent, out_weight)


def rms_rows(row_data, row_gain):
    values = row_data.astype(f32)
    scaled = values * lax.rsqrt(jnp.mean(values * values, axis=-1, keepdims=True) + epsilon)
    return scaled * row_gain


def project(matrix, weight):
    return jnp.dot(matrix, weight, preferred_element_type=f32).astype(bf16)


def running_sums(log_decay, size):
    parts = log_decay.reshape((-1, size) + log_decay.shape[1:])
    lower = jnp.tril(jnp.ones((size, size), f32))
    ahead = jnp.einsum("ij,njh->nih", lower, parts[:, :, 0], precision=lax.Precision.HIGHEST)
    behind = jnp.einsum("ji,njh->nih", lower, parts[:, :, 1], precision=lax.Precision.HIGHEST)
    return jnp.stack([ahead, behind], axis=2).reshape(log_decay.shape)


def body(
    latent,
    context,
    condition,
    context_condition,
    shift_weight,
    scale_weight,
    gate_weight,
    norm_gain,
    query_weight,
    key_weight,
    value_weight,
    write_weight,
    decay_weight,
    write_bias,
    decay_bias,
    log_rate,
    head_gain,
    out_weight,
):
    heads_here = query_weight.shape[1] // HEAD_DIM
    first_head = lax.axis_index("tp") * heads_here
    tokens, ctx_tokens = latent.shape[0], context.shape[0]
    stacked = jnp.stack([condition, context_condition]).astype(f32)
    silu_rows = jax.nn.silu(stacked).astype(bf16)
    rows, gate_row = modulation(silu_rows, shift_weight, scale_weight, gate_weight)

    def modulate(row_data, row_index):
        normed = rms_rows(row_data, norm_gain)
        return (normed * (1.0 + rows[2 + row_index]) + rows[row_index]).astype(bf16)

    modulated = jnp.concatenate([modulate(latent, 0), modulate(context, 1)], axis=0)

    def own_heads(array):
        return lax.dynamic_slice_in_dim(array, first_head, heads_here, array.ndim - 1)

    gate_weights = jnp.concatenate(
        [
            own_heads(write_weight).reshape(write_weight.shape[0], -1),
            own_heads(decay_weight).reshape(decay_weight.shape[0], -1),
        ],
        axis=1,
    )
    queries = project(modulated, query_weight)
    keys = project(modulated, key_weight)
    values = project(modulated, value_weight)
    pre = project(modulated, gate_weights).astype(f32).reshape(-1, 2, 2, heads_here)
    rate = jax.nn.sigmoid(pre[:, 0] + own_heads(write_bias))
    log_decay = -jnp.exp(own_heads(log_rate)) * jax.nn.softplus(pre[:, 1] + own_heads(decay_bias))
    lat, ctx = spans(tokens, ctx_tokens)
    running = jnp.concatenate(
        [running_sums(log_decay[:tokens], lat[0][1]), running_sums(log_decay[tokens:], ctx[0][1])], axis=0
    )
    gates = jnp.stack([rate, running], axis=2)
    col = jnp.transpose(gates, (3, 0, 1, 2)).reshape(heads_here, tokens + ctx_tokens, 4)
    row = jnp.transpose(gates, (3, 1, 2, 0)).reshape(heads_here, 4, tokens + ctx_tokens)
    head_out = exchange(queries, keys, values, col, row, head_gain[None, :], tokens, ctx_tokens)
    return output(head_out, gate_row, latent, out_weight)


def solution(mesh):
    placed = (
        P("sp", None),
        P("sp", None),
        P("sp"),
        P("sp"),
        P("sp", "tp"),
        P("sp", "tp"),
        P("sp", "tp"),
        P(),
        P(None, "tp"),
        P(None, "tp"),
        P(None, "tp"),
        P(),
        P(),
        P(),
        P(),
        P(),
        P(),
        P(None, "tp"),
    )
    return jax.shard_map(body, mesh=mesh, in_specs=placed, out_specs=P("sp", "tp"), check_vma=False)
```

profile of v0, /device:TPU:0, one launch (start us, length us, event | category | flops | bytes accessed | tf_op | source)
XLA Modules:
  0.0 111.1 jit_solution(16881405424011341402)
XLA Ops:
  0.0 1.3 %fusion.6 = f32[64]{0:T(128)S(1)} fusion(bf16[64,4096]{1,0:T(8,128)(2,1)} %param.19), kind=kLoop, calls=%fused_computation.19 | loop fusion | flops 786368 | bytes 524544 | tf_op jit(solution)/shard_map/reduce_sum | solution.py:489
  1.3 0.8 fusion.41
  2.1 0.7 stack.34
  2.8 0.7 stack.35
  3.5 3.1 %fusion = f32[512]{0:T(512)S(1)} fusion(bf16[512,4096]{1,0:T(8,128)(2,1)} %latent_ref.1), kind=kLoop, calls=%fused_computation.2 | loop fusion | flops 6290944 | bytes 4196352 | tf_op jit(solution)/shard_map/reduce_sum | solution.py:489
  6.6 0.1 constant_dynamic-slice_fusion
  6.7 0.6 pad.4.silu_ref
  7.3 17.2 %modulation.1 = (f32[4,4096]{1,0:T(4,128)}, f32[1,1024]{1,0:T(1,128)}) custom-call(bf16[8,512]{1,0:T(8,128)(2,1)} %pad.4.silu_ref, bf16[512,1024]{1,0:T(8,128)(2,1)} %shift_ref.1, bf16[512,1024]{1,0:T(8,128)(2,1)} %scale_ref.1, bf16[512,1024]{1,0:T(8,128)(2,1)} %gate_ref.1), custom_call_target="tpu_custom_call" | custom-call | tf_op jit(solution)/shard_map/modulation/pallas_call | solution.py:212
  24.5 1.1 slice_add_fusion.1
  25.6 1.0 constant_dynamic-slice_fusion.3
  26.7 0.3 fusion.10
  27.0 4.1 %fusion.4 = bf16[512,4096]{1,0:T(8,128)(2,1)S(1)} fusion(bf16[512,4096]{1,0:T(8,128)(2,1)} %latent_ref.1, f32[4096]{0:T(1024)S(1)} %bitcast.85, f32[4096]{0:T(1024)S(1)} %bitcast.84, f32[4096]{0:T(1024)S(1)} %copy-done.5, f32[512]{0:T(512)S(1)} %add_rsqrt_fusion), kind=kLoop, calls=%fused_computation.6 | loop fusion | flops 12582912 | bytes 8439808 | tf_op jit(solution)/shard_map/convert_element_type | solution.py:534
  31.1 1.9 %copy-done.2 = bf16[512,4096]{1,0:T(8,128)(2,1)} copy-done((bf16[512,4096]{1,0:T(8,128)(2,1)}, bf16[512,4096]{1,0:T(8,128)(2,1)S(1)}, u32[]{:S(2)}) %copy-start.2) | copy-done | bytes 4194328
  33.0 1.3 %fusion.5 = f32[576,16]{0,1:T(8,128)S(1)} fusion(bf16[4096,8]{0,1:T(8,128)(2,1)S(1)} %reshape.85, bf16[4096,8]{0,1:T(8,128)(2,1)S(1)} %reshape.84, bf16[64,4096]{1,0:T(8,128)(2,1)S(1)} %fusion.10, bf16[512,4096]{1,0:T(8,128)(2,1)S(1)} %fusion.4), kind=kOutput, calls=%fused_computation.14 | convolution fusion | flops 85215232 | bytes 4886528 | tf_op jit(solution)/shard_map/dot_general | solution.py:494
  34.4 0.1 fusion.26
  34.5 0.1 fusion.32
  34.6 0.1 convolution_bitcast_fusion.2
  34.7 0.2 convolution_bitcast_fusion.3
  34.9 0.2 convolution_bitcast_fusion
  35.1 0.2 convolution_bitcast_fusion.1
  35.5 0.0 copy-start.8
  35.5 6.2 %convolution_convert_fusion.1.k_ref = bf16[576,512]{1,0:T(8,128)(2,1)S(1)} fusion(bf16[4096,512]{1,0:T(8,128)(2,1)} %param.27, bf16[64,4096]{1,0:T(8,128)(2,1)S(1)} %fusion.10, bf16[512,4096]{1,0:T(8,128)(2,1)} %copy-done.2), kind=kOutput, calls=%fused_computation.9 | convolution fusion | flops 2425651200 | bytes 9502720 | tf_op jit(solution)/shard_map/dot_general | solution.py:494
  41.7 0.0 copy-start.9
  41.7 2.6 %convolution_convert_fusion.v_ref = bf16[576,512]{1,0:T(8,128)(2,1)S(1)} fusion(bf16[4096,512]{1,0:T(8,128)(2,1)S(1)} %copy-done.8, bf16[64,4096]{1,0:T(8,128)(2,1)S(1)} %fusion.10, bf16[512,4096]{1,0:T(8,128)(2,1)S(1)} %copy-done.3), kind=kOutput, calls=%fused_computation.8 | convolution fusion | flops 2425651200 | bytes 9502720 | tf_op jit(solution)/shard_map/dot_general | solution.py:494
  44.3 0.0 copy-start.1
  44.4 2.6 %convolution_convert_fusion.2.q_ref = bf16[576,512]{1,0:T(8,128)(2,1)S(1)} fusion(bf16[4096,512]{1,0:T(8,128)(2,1)S(1)} %copy-done.9, bf16[64,4096]{1,0:T(8,128)(2,1)S(1)} %fusion.10, bf16[512,4096]{1,0:T(8,128)(2,1)S(1)} %copy-done.3), kind=kOutput, calls=%fused_computation.10 | convolution fusion | flops 2425651200 | bytes 9502720 | tf_op jit(solution)/shard_map/dot_general | solution.py:494
  46.9 0.4 copy.25.col_ref
  47.4 43.2 %exchange.1.head_ref = bf16[512,512]{1,0:T(8,128)(2,1)S(1)} custom-call(bf16[576,512]{1,0:T(8,128)(2,1)S(1)} %convolution_convert_fusion.2.q_ref, bf16[576,512]{1,0:T(8,128)(2,1)S(1)} %convolution_convert_fusion.1.k_ref, bf16[576,512]{1,0:T(8,128)(2,1)S(1)} %convolution_convert_fusion.v_ref, f32[4,576,4]{2,1,0:T(8,128)S(1)} %copy.25.col_ref, ...), custom_call_target="tpu_custom_call" | custom-call | tf_op jit(solution)/shard_map/exchange/pallas_call | solution.py:359
  90.6 0.0 copy-start
  90.6 0.8 copy-done
  91.4 17.5 %output.1 = bf16[512,1024]{1,0:T(8,128)(2,1)} custom-call(bf16[512,512]{1,0:T(8,128)(2,1)} %copy-done, f32[1,1024]{1,0:T(1,128)} %get-tuple-element.8.gate_ref, bf16[512,4096]{1,0:T(8,128)(2,1)} %latent_ref.1, bf16[2048,1024]{1,0:T(8,128)(2,1)} %weight_ref.1), custom_call_target="tpu_custom_call" | custom-call | tf_op jit(solution)/shard_map/output/pallas_call | solution.py:462
  108.9 2.3 %copy.27 = bf16[512,1024]{1,0:T(8,128)(2,1)} copy(bf16[512,1024]{1,0:T(8,128)(2,1)} %output.1) | data formatting | bytes 2097152
  (28 shorter events, 0.2 us)
Async XLA Ops:
  0.0 6.6 %copy-start.6 = (f32[2,16]{1,0:T(2,128)S(1)}, f32[2,16]{1,0:T(2,128)}, u32[]{:S(2)}) copy-start(f32[2,16]{1,0:T(2,128)} %param.32) | copy-start | bytes 388
  0.0 6.6 %copy-start.7 = (f32[2,16]{1,0:T(2,128)S(1)}, f32[2,16]{1,0:T(2,128)}, u32[]{:S(2)}) copy-start(f32[2,16]{1,0:T(2,128)} %param.31) | copy-start | bytes 388
  0.0 26.7 %copy-start.4 = (bf16[64,4096]{1,0:T(8,128)(2,1)S(1)}, bf16[64,4096]{1,0:T(8,128)(2,1)}, u32[]{:S(2)}) copy-start(bf16[64,4096]{1,0:T(8,128)(2,1)} %param.19) | copy-start | bytes 1572868
  0.0 26.7 %copy-start.5 = (f32[4096]{0:T(1024)S(1)}, f32[4096]{0:T(1024)}, u32[]{:S(2)}) copy-start(f32[4096]{0:T(1024)} %param.25) | copy-start | bytes 49156
  31.1 1.9 %copy-start.2 = (bf16[512,4096]{1,0:T(8,128)(2,1)}, bf16[512,4096]{1,0:T(8,128)(2,1)S(1)}, u32[]{:S(2)}) copy-start(bf16[512,4096]{1,0:T(8,128)(2,1)S(1)} %fusion.4) | copy-start | bytes 12582916
  35.5 6.2 %copy-start.3 = (bf16[512,4096]{1,0:T(8,128)(2,1)S(1)}, bf16[512,4096]{1,0:T(8,128)(2,1)}, u32[]{:S(2)}) copy-start(bf16[512,4096]{1,0:T(8,128)(2,1)} %copy-done.2) | copy-start | bytes 12582916
  35.5 6.2 %copy-start.8 = (bf16[4096,512]{1,0:T(8,128)(2,1)S(1)}, bf16[4096,512]{1,0:T(8,128)(2,1)}, u32[]{:S(2)}) copy-start(bf16[4096,512]{1,0:T(8,128)(2,1)} %param.28) | copy-start | bytes 12582916
  41.7 2.6 %copy-start.9 = (bf16[4096,512]{1,0:T(8,128)(2,1)S(1)}, bf16[4096,512]{1,0:T(8,128)(2,1)}, u32[]{:S(2)}) copy-start(bf16[4096,512]{1,0:T(8,128)(2,1)} %param.26) | copy-start | bytes 12582916
  44.3 3.0 %copy-start.1 = (f32[128]{0:T(128)S(1)}, f32[128]{0:T(128)}, u32[]{:S(2)}) copy-start(f32[128]{0:T(128)} %param.34) | copy-start | bytes 1540
  90.6 0.8 copy-start
where the time goes:
time: 112 us; the launch traced here: 111 us
  Pallas kernels  78 us (70%)
  matrix products  13.4 us (12%)
  other arithmetic  10.8 us (10%)
  local copies, waits for them, and re-layouts  8.67 us (8%)
    pallas_call x1, Pallas kernels, exchange(): pl.pallas_call(functools.partial(exchange_kernel, sp, per, tokens, ctx_to...  43.2 us
    pallas_call x1, Pallas kernels, output(): pl.pallas_call(functools.partial(output_kernel, tp, pieces), in_specs=[vm...  17.5 us
    pallas_call x1, Pallas kernels, modulation(): pl.pallas_call(functools.partial(modulation_kernel, sp, tp), in_specs=[vm...  17.2 us
    dot_general x4, matrix products, project(): return jnp.dot(matrix, weight, preferred_element_type=f32).astype(bf16)  12.7 us
    unnamed x21, local copies, waits for them, and re-layouts  5.03 us
    reduce_sum x2, other arithmetic, rms_rows(): jnp.mean(values * values, axis=-1, keepdims=True) + epsilon  4.4 us
    convert_element_type x2, other arithmetic, modulate(): return (normed * (1.0 + rows[2 + row_index]) + rows[row_index]).astype(bf16)  4.33 us

commit v1 on v0

v1 whole, which is shorter than its diff:
```python
import functools

import jax
import jax.numpy as jnp
from jax import lax
from jax.experimental import pallas as pl
from jax.experimental.pallas import tpu as pltpu
from jax.sharding import PartitionSpec as P

HEAD_DIM = 128
CHUNK = 128
epsilon = 0.0001
bf16 = jnp.bfloat16
f32 = jnp.float32


def mm(a, b):
    return jnp.dot(a.astype(bf16), b.astype(bf16), preferred_element_type=f32)


def on_mesh(sp=None, tp=None):
    return (lax.axis_index("sp") if sp is None else sp, lax.axis_index("tp") if tp is None else tp)


def send(src, dst, send_sem, recv_sem, device):
    return pltpu.make_async_remote_copy(
        src_ref=src,
        dst_ref=dst,
        send_sem=send_sem,
        recv_sem=recv_sem,
        device_id=device,
        device_id_type=pl.DeviceIdType.MESH,
    )


def greet(devices):
    barrier = pltpu.get_barrier_semaphore()
    for device in devices:
        pl.semaphore_signal(barrier, inc=1, device_id=device, device_id_type=pl.DeviceIdType.MESH)


def grid_iota(size):
    return (
        lax.broadcasted_iota(jnp.int32, (size, size), 0),
        lax.broadcasted_iota(jnp.int32, (size, size), 1),
    )


def start_inverse(item, rows, cols):
    near = (rows // 2) == (cols // 2)
    item["inv"] = jnp.where(rows == cols, 1.0, jnp.where(near, -item["system"], 0.0))


def finish_inverse(items, size):
    span = 2
    while span < size:
        firsts = []
        for item in items:
            late, early = item["late_axis"] // span, item["early_axis"] // span
            mask = ((late % 2) == 1) & (early == late - 1)
            firsts.append(mm(jnp.where(mask, item["system"], 0.0), item["inv"]))
        for item, first in zip(items, firsts):
            item["inv"] = item["inv"] - mm(item["inv"], first)
        span *= 2


def key_grams(keys):
    size = keys.shape[0]
    rows, cols = grid_iota(size)
    keys_t = keys.astype(f32).T
    gram = jnp.dot(keys, keys_t.astype(bf16), preferred_element_type=f32)
    diag = jnp.where(rows == cols, gram, 0.0)
    s_col = lax.rsqrt(jnp.sum(diag, axis=1, keepdims=True) + epsilon)
    s_row = lax.rsqrt(jnp.sum(diag, axis=0, keepdims=True) + epsilon)
    return gram * s_col * s_row, keys.astype(f32) * s_col, keys_t * s_row, s_row


def eye_matrix():
    rows, cols = grid_iota(HEAD_DIM)
    return (rows == cols).astype(f32)


def prepare_maps(tokens, span, k_ref, v_ref, col_ref, row_ref, srow_ref, solved_ref, carry_ref, map_ref):
    size = min(CHUNK, tokens)
    rows, cols = grid_iota(size)
    items = []
    shared = []
    for at in range(0, tokens, size):
        gram, keys, keys_t, s_row = key_grams(k_ref[at : at + size, :])
        srow_ref[:, at : at + size] = s_row
        shared.append((keys, keys_t, v_ref[at : at + size, :].astype(f32)))
        for d in range(2):
            rate_col = col_ref[at : at + size, span * d : span * d + 1]
            run_col = col_ref[at : at + size, span * (2 + d) : span * (2 + d) + 1]
            run_row = row_ref[2 + d : 3 + d, at : at + size]
            strict = rows > cols if d == 0 else rows < cols
            decay = jnp.where(strict, jnp.exp(jnp.minimum(run_col - run_row, 0.0)), 0.0)
            item = dict(at=at, d=d, rate_col=rate_col, run_col=run_col, run_row=run_row)
            item["system"] = gram * decay * rate_col
            item["late_axis"], item["early_axis"] = (rows, cols) if d == 0 else (cols, rows)
            start_inverse(item, rows, cols)
            items.append(item)
    finish_inverse(items, size)
    for item in items:
        keys, keys_t, values = shared[item["at"] // size]
        growth = jnp.exp(item["run_col"])
        both = jnp.concatenate([values * item["rate_col"], keys * (item["rate_col"] * growth)], axis=1)
        solved = mm(item["inv"], both).astype(bf16)
        solved_ref[item["at"] // size, item["d"]] = solved
        last = item["run_row"][:, size - 1 :] if item["d"] == 0 else item["run_row"][:, :1]
        item["gate"] = jnp.exp(last)
        item["late"] = mm(keys_t * jnp.exp(last - item["run_row"]), solved)
    eye = eye_matrix()
    for d in range(2):
        chunks = [i for i in items if i["d"] == d]
        carry = None
        for item in chunks if d == 0 else chunks[::-1]:
            late, gate = item["late"], item["gate"]
            fresh = jnp.concatenate([late[:, :HEAD_DIM], (gate - 1.0) * eye - late[:, HEAD_DIM:]], axis=1)
            if carry is None:
                carry = fresh
            else:
                held = carry.astype(bf16)
                carry_ref[item["at"] // size, d] = held
                carry = gate * carry + fresh - mm(late[:, HEAD_DIM:], held)
        map_ref[d] = carry.astype(bf16)


def prepare_outputs(tokens, span, q_ref, k_ref, col_ref, row_ref, srow_ref, solved_ref, carry_ref, o_ref, e_ref):
    size = min(CHUNK, tokens)
    rows, cols = grid_iota(size)
    count = tokens // size
    for index in range(count):
        at = index * size
        raw = q_ref[at : at + size, :]
        queries = raw.astype(f32)
        q_scale = lax.rsqrt(jnp.sum(queries * queries, axis=1, keepdims=True) + epsilon) * HEAD_DIM**-0.5
        queries = queries * q_scale
        score = lax.dot_general(
            raw, k_ref[at : at + size, :], (((1,), (1,)), ((), ())), preferred_element_type=f32
        ) * (q_scale * srow_ref[:, at : at + size])
        total = None
        for d in range(2):
            run_col = col_ref[at : at + size, span * (2 + d) : span * (2 + d) + 1]
            run_row = row_ref[2 + d : 3 + d, at : at + size]
            inside = rows >= cols if d == 0 else rows <= cols
            decay = jnp.where(inside, jnp.exp(jnp.minimum(run_col - run_row, 0.0)), 0.0)
            weighed = mm(score * decay, solved_ref[index, d])
            local = weighed[:, :HEAD_DIM]
            early = queries * jnp.exp(run_col) - weighed[:, HEAD_DIM:]
            if index != (0 if d == 0 else count - 1):
                moved = mm(early, carry_ref[index, d])
                local = local + moved[:, :HEAD_DIM]
                early = early + moved[:, HEAD_DIM:]
            e_ref[at : at + size, d * HEAD_DIM : (d + 1) * HEAD_DIM] = early.astype(bf16)
            total = local if total is None else total + local
        o_ref[at : at + size, :] = total


def context_state(places, d, k_ref, v_ref, g_ref):
    size = k_ref.shape[1]
    rows, cols = grid_iota(size)
    items = []
    for step in range(places):
        place = step + d * (places - 1 - 2 * step)
        gram, keys, keys_t, unused = key_grams(k_ref[place])
        gates = g_ref[place]
        gates_t = gates.T
        rate_col, run_col, run_row = gates_t[:size, 0:1], gates_t[:size, 1:2], gates[1:2, :size]
        item = dict(keys=keys, keys_t=keys_t, values=v_ref[place].astype(f32), rate_col=rate_col)
        item["run_col"], item["run_row"] = run_col, run_row
        item["late_axis"] = jnp.where(d == 0, rows, cols)
        item["early_axis"] = jnp.where(d == 0, cols, rows)
        strict = item["late_axis"] > item["early_axis"]
        decay = jnp.where(strict, jnp.exp(jnp.minimum(run_col - run_row, 0.0)), 0.0)
        item["system"] = gram * decay * rate_col
        start_inverse(item, rows, cols)
        items.append(item)
    finish_inverse(items, size)
    for item in items:
        growth = jnp.exp(item["run_col"])
        both = jnp.concatenate(
            [item["values"] * item["rate_col"], item["keys"] * (item["rate_col"] * growth)], axis=1
        )
        solved = mm(item["inv"], both)
        run_row = item["run_row"]
        last = jnp.where(d == 0, run_row[:, size - 1 :], run_row[:, :1])
        item["gate"] = jnp.exp(last)
        item["late"] = mm(item["keys_t"] * jnp.exp(last - run_row), solved)
    state = items[0]["late"][:, :HEAD_DIM]
    for item in items[1:]:
        late = item["late"]
        state = item["gate"] * state + late[:, :HEAD_DIM] - mm(late[:, HEAD_DIM:], state)
    return state


def log1p_unit(u):
    z = u / (2.0 + u)
    z2 = z * z
    series = 1.0 / 11.0 + 0.0 * z2
    for power in (9, 7, 5, 3, 1):
        series = series * z2 + 1.0 / power
    return 2.0 * z * series


def triangle_sums(lower, parts):
    return sum(jnp.dot(lower, part, preferred_element_type=f32) for part in parts)


def split_three(values):
    high = values.astype(bf16)
    rest = values - high.astype(f32)
    middle = rest.astype(bf16)
    return high, middle, (rest - middle.astype(f32)).astype(bf16)


def mixer_kernel(
    sp, tp, heads, per,
    cond_ref, ctx_cond_ref, gain_ref, head_gain_ref, wb_ref, db_ref, lr_ref,
    shift_ref, scale_ref, gate_ref, latent_ref, context_ref, write_ref, decay_ref,
    wq_ref, wk_ref, wv_ref, wo_ref,
    out_ref,
    mod_w, rows_in, weights, gate_w, wo, rstd, mixed, q_s, k_s, v_s,
    got, blocks, gate_row, cols, rows_g, srow, solved, carry, maps, o_s, e_s,
    ctx_send, ctx_k, ctx_v, ctx_g, s_zero, got_map, pair_map, start_in, start_own, hop_out, ho, acc,
    local_sems, sent_a, recv_a, sent_b, recv_b, sent_c, recv_c, sent_s, recv_s, sent_m, recv_m,
    sent_h, sent_y, recv_y, sent_p, recv_p, sent_r, recv_r,
):
    me, col = lax.axis_index("sp"), lax.axis_index("tp")
    width = shift_ref.shape[1]
    tokens, ctx_tokens = latent_ref.shape[0], context_ref.shape[0]
    total_rows = tokens + ctx_tokens
    depth = latent_ref.shape[1]
    out_width = heads * HEAD_DIM
    items = 2 * heads
    loads = []

    def load(src, dst):
        loads.append(pltpu.make_async_copy(src, dst, local_sems.at[len(loads)]))
        loads[-1].start()
        return loads[-1]

    mods = [load(ref, mod_w.at[i]) for i, ref in enumerate([shift_ref, scale_ref, gate_ref])]
    acts = [
        load(context_ref, rows_in.at[pl.ds(tokens, ctx_tokens)]),
        load(latent_ref, rows_in.at[pl.ds(0, tokens)]),
    ]
    gate_rows = write_ref.shape[0]
    projs = [
        load(write_ref, gate_w.at[pl.ds(0, gate_rows)]),
        load(decay_ref, gate_w.at[pl.ds(gate_rows, gate_rows)]),
    ]
    projs += [
        load(ref, weights.at[:, pl.ds(i * out_width, out_width)]) for i, ref in enumerate([wk_ref, wv_ref, wq_ref])
    ]
    out_load = load(wo_ref, wo)
    rings = [on_mesh(sp=lax.rem(me + r, sp)) for r in range(1, sp)]
    cross = [on_mesh(tp=lax.rem(col + r, tp)) for r in range(1, tp)]
    greet(rings + cross)

    def flat(ref):
        values = ref[...].astype(f32)
        return jnp.concatenate([values[i : i + 1] for i in range(values.shape[0])], axis=1)

    silu = jnp.concatenate([flat(cond_ref), flat(ctx_cond_ref), jnp.zeros((6, cond_ref.size), f32)], axis=0)
    silu = (silu / (1.0 + jnp.exp(-silu))).astype(bf16)
    parts = []
    for i in range(3):
        mods[i].wait()
        parts.append(jnp.dot(silu, mod_w[i], preferred_element_type=f32))
    got[me] = jnp.concatenate(
        [parts[0][0:2], parts[1][0:2], parts[2][0:1], jnp.zeros((3, width), f32)], axis=0
    ).astype(bf16)
    pl.semaphore_wait(pltpu.get_barrier_semaphore(), len(rings) + len(cross))
    out = []
    for r, device in enumerate(rings):
        out.append(send(got.at[me], got.at[me], sent_a.at[r], recv_a.at[me], device))
        out[-1].start()
    for act in acts:
        act.wait()
    step = 16

    def stats(i, unused):
        at = pl.ds(pl.multiple_of(i * step, step), step)
        values = rows_in[at, :].astype(f32)
        mean = jnp.sum(values * values, axis=1, keepdims=True) * (1.0 / depth)
        rstd[at, :] = jnp.broadcast_to(lax.rsqrt(mean + epsilon), (step, 128))
        return unused

    lax.fori_loop(0, total_rows // step, stats, 0)
    for r in range(1, sp):
        src = lax.rem(me + r, sp)
        send(got.at[src], got.at[src], sent_a.at[0], recv_a.at[src], on_mesh(sp=src)).wait_recv()
    summed = got[0].astype(f32)
    for place in range(1, sp):
        summed = summed + got[place].astype(f32)
    blocks[col] = summed[0:4]
    gate_row[...] = summed[4:5]
    for r, device in enumerate(cross):
        out.append(send(blocks.at[col], blocks.at[col], sent_b.at[r], recv_b.at[col], device))
        out[-1].start()
    for r in range(1, tp):
        src = lax.rem(col + r, tp)
        send(blocks.at[src], blocks.at[src], sent_b.at[0], recv_b.at[src], on_mesh(tp=src)).wait_recv()

    def modulate_rows(start, count, index):
        for place in range(tp):
            lanes = slice(place * width, (place + 1) * width)
            block = blocks[place]
            slope = gain_ref[:, lanes] * (1.0 + block[2 + index : 3 + index])
            shift = block[index : index + 1]

            def modulate(i, unused):
                at = pl.ds(pl.multiple_of(start + i * step, step), step)
                scale = jnp.concatenate([rstd[at, :]] * (width // 128), axis=1)
                mixed[at, lanes] = (rows_in[at, lanes].astype(f32) * scale * slope + shift).astype(bf16)
                return unused

            lax.fori_loop(0, count // step, modulate, 0)

    tile = 256 if out_width % 256 == 0 else 128

    def project(first, count, which, ref, base):
        def columns(j, unused):
            lanes = pl.ds(pl.multiple_of(which * out_width + j * tile, tile), tile)
            part = jnp.dot(mixed[pl.ds(first, count), :], weights[:, lanes], preferred_element_type=f32)
            ref[pl.ds(first, count), pl.ds(pl.multiple_of(j * tile, tile), tile)] = part.astype(bf16)
            return unused

        lax.fori_loop(0, out_width // tile, columns, 0)

    first_head = col * heads
    span = wb_ref.shape[1]
    bias = jnp.concatenate([wb_ref[0:1], wb_ref[1:2], db_ref[0:1], db_ref[1:2]], axis=1)
    rates = jnp.concatenate([lr_ref[0:1], lr_ref[1:2]] * 2, axis=1)
    lanes_here = bias.shape[1]

    def make_gates(first, count, size):
        pre = lax.dot_general(
            mixed[pl.ds(first, count), :], gate_w[...], (((1,), (1,)), ((), ())), preferred_element_type=f32
        ).astype(bf16).astype(f32) + bias
        rate = 1.0 / (1.0 + jnp.exp(-pre))
        decay = -jnp.exp(rates) * (jnp.maximum(pre, 0.0) + log1p_unit(jnp.exp(-jnp.abs(pre))))
        lane = lax.broadcasted_iota(jnp.int32, (count, lanes_here), 1)
        rows, columns = grid_iota(size)
        lower, upper = (rows >= columns).astype(bf16), (rows <= columns).astype(bf16)
        backward = lax.broadcasted_iota(jnp.int32, (size, lanes_here), 1) >= 3 * span
        running = []
        for at in range(0, count, size):
            split = split_three(decay[at : at + size])
            running.append(jnp.where(backward, triangle_sums(upper, split), triangle_sums(lower, split)))
        gates = jnp.where(lane < 2 * span, rate, jnp.concatenate(running, axis=0))
        gates = jnp.concatenate([gates, jnp.zeros((count, 128 - lanes_here), f32)], axis=1)
        gates = pltpu.roll(gates, lax.rem(128 - first_head, 128), 1)
        for head in range(heads):
            cols[head, pl.ds(first, count), :] = gates if head == 0 else pltpu.roll(gates, 128 - head, 1)
        return gates

    for proj in projs[:2]:
        proj.wait()
    modulate_rows(tokens, ctx_tokens, 1)
    ctx_gates = make_gates(tokens, ctx_tokens, ctx_tokens)
    if ctx_tokens < 128:
        ctx_gates = jnp.concatenate([ctx_gates, jnp.zeros((128 - ctx_tokens, 128), f32)], axis=0)
    gates_t = ctx_gates.T
    for item in range(items):
        head, d = item // 2, item % 2
        ctx_send[item] = jnp.concatenate(
            [
                gates_t[span * d + head : span * d + head + 1],
                gates_t[span * (2 + d) + head : span * (2 + d) + head + 1],
                jnp.zeros((6, 128), f32),
            ],
            axis=0,
        )
    for proj in projs[2:4]:
        proj.wait()
    project(tokens, ctx_tokens, 0, k_s, 0)
    project(tokens, ctx_tokens, 1, v_s, 0)

    def ctx_copies(item, place, slot, device):
        lanes = pl.ds((item // 2) * HEAD_DIM, HEAD_DIM)
        at = pl.ds(tokens, ctx_tokens)
        pairs = [
            (k_s.at[at, lanes], ctx_k.at[slot, place]),
            (v_s.at[at, lanes], ctx_v.at[slot, place]),
            (ctx_send.at[item], ctx_g.at[slot, place]),
        ]
        return [
            send(src, dst, sent_c.at[item, j], recv_c.at[slot, place, j], device) for j, (src, dst) in enumerate(pairs)
        ]

    for item in range(items):
        owner, slot = item // per, item % per

        @pl.when(owner != me)
        def _():
            for copy in ctx_copies(item, me, slot, on_mesh(sp=owner)):
                copy.start()

        @pl.when(owner == me)
        def _():
            lanes = slice((item // 2) * HEAD_DIM, (item // 2 + 1) * HEAD_DIM)
            ctx_k[slot, me] = k_s[tokens : tokens + ctx_tokens, lanes]
            ctx_v[slot, me] = v_s[tokens : tokens + ctx_tokens, lanes]
            ctx_g[slot, me] = ctx_send[item]

    modulate_rows(0, tokens, 0)
    size = min(CHUNK, tokens)
    gates = make_gates(0, tokens, size)
    for at in range(0, tokens, 128):
        block_t = gates[at : at + 128].T
        for head in range(heads):
            rows_g[head, :, at : at + 128] = jnp.concatenate(
                [
                    block_t[base + head : base + head + 1] for base in range(0, 4 * span, span)
                ]
                + [jnp.zeros((4, 128), f32)],
                axis=0,
            )
    project(0, tokens, 0, k_s, 0)
    project(0, tokens, 1, v_s, 0)
    projs[4].wait()
    project(0, tokens, 2, q_s, 0)

    blocks_here = sp // 2
    one_way = lax.rem(me + 1, 2)
    other_way = 1 - one_way

    def lanes_of(head):
        return pl.ds(pl.multiple_of(head * HEAD_DIM, HEAD_DIM), HEAD_DIM)

    def map_copy(head, towards):
        d = other_way
        return send(
            maps.at[head, d], got_map.at[head], sent_m.at[head], recv_m.at[head], on_mesh(sp=me + towards)
        )

    out_step = 1 - 2 * other_way
    in_step = 1 - 2 * one_way

    def stage_a(head):
        lanes = lanes_of(head)
        prepare_maps(
            tokens,
            span,
            k_s.at[:, lanes],
            v_s.at[:, lanes],
            cols.at[head],
            rows_g.at[head],
            srow.at[head],
            solved.at[head],
            carry.at[head],
            maps.at[head],
        )
        map_copy(head, out_step).start()

    def stage_b(head):
        lanes = lanes_of(head)
        prepare_outputs(
            tokens,
            span,
            q_s.at[:, lanes],
            k_s.at[:, lanes],
            cols.at[head],
            rows_g.at[head],
            srow.at[head],
            solved.at[head],
            carry.at[head],
            o_s.at[head],
            e_s.at[head],
        )

    def stage_pair(head):
        map_copy(head, -in_step).wait_recv()
        theirs, mine = got_map[head], maps[head, one_way]
        pair_map[head] = (
            theirs.astype(f32)
            + mine.astype(f32)
            + jnp.dot(mine[:, HEAD_DIM:], theirs, preferred_element_type=f32)
        )

    def first_devices(d):
        return [d * (sp - 1) + (1 - 2 * d) * i for i in range(2)]

    def zero_copy(slot, item, j):
        head, d = item // 2, lax.rem(item, 2)
        return first_devices(d)[j], send(
            s_zero.at[slot],
            start_in.at[head, d],
            sent_s.at[slot, j],
            recv_s.at[head, d],
            on_mesh(sp=first_devices(d)[j]),
        )

    def stage_context():
        for slot in range(per):
            item = me * per + slot

            @pl.when(item < items)
            def _():
                for r in range(1, sp):
                    src = lax.rem(me + r, sp)
                    for j, spot in enumerate((ctx_k.at[slot, src], ctx_v.at[slot, src], ctx_g.at[slot, src])):
                        send(spot, spot, sent_c.at[0, j], recv_c.at[slot, src, j], on_mesh(sp=src)).wait_recv()
                state = context_state(sp, lax.rem(item, 2), ctx_k.at[slot], ctx_v.at[slot], ctx_g.at[slot])
                s_zero[slot] = state.astype(bf16)
                for j in range(2):
                    device, copy = zero_copy(slot, item, j)

                    @pl.when(device != me)
                    def _():
                        copy.start()

                    @pl.when(device == me)
                    def _():
                        start_in[item // 2, lax.rem(item, 2)] = state.astype(bf16)

    def rank_block(d):
        return (d * (sp - 1) + (1 - 2 * d) * me) // 2

    def hop_copy(head, j):
        d = one_way
        return send(
            hop_out.at[head],
            start_in.at[head, d],
            sent_h.at[head, j],
            recv_s.at[head, d],
            on_mesh(sp=me + in_step * (2 - j)),
        )

    def stage_state(head, d):
        block = rank_block(d)
        owner = (2 * head + d) // per

        @pl.when((block > 0) | (owner != me))
        def _():
            spot = start_in.at[head, d]
            send(spot, spot, sent_h.at[head, 0], recv_s.at[head, d], on_mesh(sp=lax.rem(me + 1, sp))).wait_recv()

        state = start_in[head, d]

        @pl.when(d == one_way)
        def _():
            @pl.when(block < blocks_here - 1)
            def _():
                pair = pair_map[head]
                hop_out[head] = (
                    state.astype(f32)
                    + pair[:, :HEAD_DIM]
                    + jnp.dot(pair[:, HEAD_DIM:].astype(bf16), state, preferred_element_type=f32)
                ).astype(bf16)
                for j in range(2):
                    hop_copy(head, j).start()

            theirs = got_map[head]
            start_own[head, d] = (
                state.astype(f32)
                + theirs[:, :HEAD_DIM].astype(f32)
                + jnp.dot(theirs[:, HEAD_DIM:], state, preferred_element_type=f32)
            ).astype(bf16)

        @pl.when(d != one_way)
        def _():
            start_own[head, d] = state

    core = lax.rem(col, 2)
    partner = col + 1 - 2 * core
    chips = tp // 2
    far = [lax.rem(col + 2 * r, tp) for r in range(1, chips)]
    far_partner = [place + 1 - 2 * core for place in far]

    def far_copy(head, r):
        spot = ho.at[col, head]
        return send(spot, spot, sent_y.at[head, r], recv_y.at[head, col], on_mesh(tp=far[r]))

    def partner_copy(head):
        spot = ho.at[col, head]
        return send(spot, spot, sent_p.at[head], recv_p.at[head], on_mesh(tp=partner))

    def relay_copy(head, r):
        spot = ho.at[far[r], head]
        return send(spot, spot, sent_r.at[head, r], recv_r.at[head, far[r]], on_mesh(tp=partner))

    def stage_final(head):
        states = jnp.concatenate([start_own[head, 0], start_own[head, 1]], axis=0)
        combined = o_s[head] + jnp.dot(e_s[head], states, preferred_element_type=f32)
        scale = lax.rsqrt(jnp.mean(combined * combined, axis=1, keepdims=True) + epsilon)
        ho[col, head] = (combined * scale * head_gain_ref[...]).astype(bf16)
        for r in range(chips - 1):
            far_copy(head, r).start()
        partner_copy(head).start()

    first_dir = jnp.where(me < sp // 2, 0, 1)
    near_block = rank_block(first_dir)
    far_block = blocks_here - 1 - near_block

    def lag(block):
        return 1 + 2 * block + jnp.where(block >= 2, 1, 0)

    def slot_events(s):
        head1 = s - lag(near_block)

        @pl.when((head1 >= 0) & (head1 < heads))
        def _():
            stage_state(head1, first_dir)

        head2 = s - lag(far_block)

        @pl.when((head2 >= 0) & (head2 < heads))
        def _():
            stage_state(head2, 1 - first_dir)
            stage_final(head2)

    def loop_a(head, unused):
        stage_a(head)

        @pl.when(head == 0)
        def _():
            stage_context()

        @pl.when(head > 0)
        def _():
            stage_pair(head - 1)

        slot_events(head)
        return unused

    lax.fori_loop(0, heads, loop_a, 0)

    def loop_b(head, unused):
        stage_b(head)

        @pl.when(head == 0)
        def _():
            stage_pair(heads - 1)

        slot_events(heads + head)
        return unused

    lax.fori_loop(0, heads, loop_b, 0)
    last_slot = heads + 1 + 2 * (blocks_here - 1) + (1 if blocks_here > 2 else 0)

    def loop_c(s, unused):
        slot_events(s)
        return unused

    lax.fori_loop(2 * heads, last_slot, loop_c, 0)
    out_load.wait()
    group = min(2, heads)

    def add(src, first, count, start):
        block = jnp.concatenate([ho[src, first + i] for i in range(count)], axis=1)

        def columns(j, unused):
            lanes = pl.ds(pl.multiple_of(j * tile, tile), tile)
            at = pl.ds(pl.multiple_of(src * out_width + first * HEAD_DIM, HEAD_DIM), count * HEAD_DIM)
            part = jnp.dot(block, wo[at, lanes], preferred_element_type=f32)
            acc[:, lanes] = part if start else acc[:, lanes] + part
            return unused

        lax.fori_loop(0, width // tile, columns, 0)

    add(col, 0, heads, True)
    for head in range(heads):
        spot = ho.at[partner, head]
        send(spot, spot, sent_p.at[head], recv_p.at[head], on_mesh(tp=partner)).wait_recv()
    add(partner, 0, heads, False)
    for first in range(0, heads, group):
        for head in range(first, first + group):
            for r, src in enumerate(far):
                spot = ho.at[src, head]
                send(spot, spot, sent_y.at[head, r], recv_y.at[head, src], on_mesh(tp=src)).wait_recv()
                relay_copy(head, r).start()
        for src in far:
            add(src, first, group, False)
        for head in range(first, first + group):
            for r, src in enumerate(far_partner):
                spot = ho.at[src, head]
                send(spot, spot, sent_r.at[head, r], recv_r.at[head, src], on_mesh(tp=partner)).wait_recv()
        for src in far_partner:
            add(src, first, group, False)

    def finish(i, unused):
        at = pl.ds(pl.multiple_of(i * step, step), step)
        residual = rows_in[at, pl.ds(pl.multiple_of(col * width, width), width)].astype(f32)
        out_ref[at, :] = (residual + gate_row[...] * acc[at, :]).astype(bf16)
        return unused

    lax.fori_loop(0, tokens // step, finish, 0)
    for copy in out:
        copy.wait_send()
    for item in range(items):
        owner, slot = item // per, item % per

        @pl.when(owner != me)
        def _():
            for copy in ctx_copies(item, me, slot, on_mesh(sp=owner)):
                copy.wait_send()

    for slot in range(per):
        item = me * per + slot

        @pl.when(item < items)
        def _():
            for j in range(2):
                device, copy = zero_copy(slot, item, j)

                @pl.when(device != me)
                def _():
                    copy.wait_send()

    for head in range(heads):
        map_copy(head, out_step).wait_send()

        @pl.when(rank_block(one_way) < blocks_here - 1)
        def _():
            for j in range(2):
                hop_copy(head, j).wait_send()

        for r in range(chips - 1):
            far_copy(head, r).wait_send()
            relay_copy(head, r).wait_send()
        partner_copy(head).wait_send()


def body(
    latent,
    context,
    condition,
    context_condition,
    shift_weight,
    scale_weight,
    gate_weight,
    norm_gain,
    query_weight,
    key_weight,
    value_weight,
    write_weight,
    decay_weight,
    write_bias,
    decay_bias,
    log_rate,
    head_gain,
    out_weight,
):
    sp, tp = lax.axis_size("sp"), lax.axis_size("tp")
    tokens, depth = latent.shape
    ctx_tokens = context.shape[0]
    rows = tokens + ctx_tokens
    out_width = query_weight.shape[1]
    heads = out_width // HEAD_DIM
    items = 2 * heads
    per = -(-items // sp)
    width = out_weight.shape[1]
    chunks = tokens // min(CHUNK, tokens)
    gate_rows = 2 * write_bias.shape[1]
    vmem = pl.BlockSpec(memory_space=pltpu.VMEM)
    anywhere = pl.BlockSpec(memory_space=pl.ANY)
    dma = pltpu.SemaphoreType.DMA
    square, wide = (HEAD_DIM, HEAD_DIM), (HEAD_DIM, 2 * HEAD_DIM)
    scratch = [
        ((3,) + shift_weight.shape, bf16),
        ((rows, depth), bf16),
        ((depth, 3 * out_width), bf16),
        ((2 * gate_rows, depth), bf16),
        (out_weight.shape, bf16),
        ((rows, 128), f32),
        ((rows, depth), bf16),
        ((tokens, out_width), bf16),
        ((rows, out_width), bf16),
        ((rows, out_width), bf16),
        ((sp, 8, width), bf16),
        ((tp, 4, width), f32),
        ((1, width), f32),
        ((heads, rows, 128), f32),
        ((heads, 8, tokens), f32),
        ((heads, 1, tokens), f32),
        ((heads, chunks, 2, tokens // chunks, 2 * HEAD_DIM), bf16),
        ((heads, chunks, 2) + wide, bf16),
        ((heads, 2) + wide, bf16),
        ((heads, tokens, HEAD_DIM), f32),
        ((heads, tokens, 2 * HEAD_DIM), bf16),
        ((items, 8, 128), f32),
        ((per, sp, ctx_tokens, HEAD_DIM), bf16),
        ((per, sp, ctx_tokens, HEAD_DIM), bf16),
        ((per, sp, 8, 128), f32),
        ((per,) + square, bf16),
        ((heads,) + wide, bf16),
        ((heads,) + wide, f32),
        ((heads, 2) + square, bf16),
        ((heads, 2) + square, bf16),
        ((heads,) + square, bf16),
        ((tp, heads, tokens, HEAD_DIM), bf16),
        ((tokens, width), f32),
    ]
    semaphores = [
        (11,), (sp,), (sp,), (tp,), (tp,), (items, 3), (per, sp, 3), (per, 2), (heads, 2), (heads,), (heads,),
        (heads, 2), (heads, tp), (heads, tp), (heads,), (heads,), (heads, tp), (heads, tp),
    ]
    return pl.pallas_call(
        functools.partial(mixer_kernel, sp, tp, heads, per),
        in_specs=[vmem] * 7 + [anywhere] * 11,
        out_specs=vmem,
        out_shape=jax.ShapeDtypeStruct((tokens, width), bf16),
        scratch_shapes=[pltpu.VMEM(shape, dtype) for shape, dtype in scratch] + [dma(shape) for shape in semaphores],
        compiler_params=pltpu.CompilerParams(
            collective_id=0, has_side_effects=True, vmem_limit_bytes=63 * 1024 * 1024
        ),
        name="mixer",
    )(
        condition.reshape(-1, 128),
        context_condition.reshape(-1, 128),
        norm_gain[None, :],
        head_gain[None, :],
        write_bias,
        decay_bias,
        log_rate,
        shift_weight,
        scale_weight,
        gate_weight,
        latent,
        context,
        jnp.transpose(write_weight, (1, 2, 0)).reshape(gate_rows, depth),
        jnp.transpose(decay_weight, (1, 2, 0)).reshape(gate_rows, depth),
        query_weight,
        key_weight,
        value_weight,
        out_weight,
    )


def solution(mesh):
    placed = (
        P("sp", None),
        P("sp", None),
        P("sp"),
        P("sp"),
        P("sp", "tp"),
        P("sp", "tp"),
        P("sp", "tp"),
        P(),
        P(None, "tp"),
        P(None, "tp"),
        P(None, "tp"),
        P(),
        P(),
        P(),
        P(),
        P(),
        P(),
        P(None, "tp"),
    )
    return jax.shard_map(body, mesh=mesh, in_specs=placed, out_specs=P("sp", "tp"), check_vma=False)
```

time: 112 us -> 76.6 us (0.68)
  matrix products: 13.4 us -> 0 us
  other arithmetic: 10.8 us -> 0 us
  local copies, waits for them, and re-layouts: 8.67 us -> 2.26 us
  Pallas kernels: 78 us -> 74.1 us
    dot_general x8 -> x0, matrix products: 13.4 us -> none  [the longest x4 12.7 us: project(): return jnp.dot(matrix, weight, preferred_element_type=f32).astype(bf16)]
    reduce_sum x2 -> x0, other arithmetic: 4.4 us -> none  [rms_rows(): jnp.mean(values * values, axis=-1, keepdims=True) + epsilon]
    convert_element_type x3 -> x0, other arithmetic: 4.35 us -> none  [the longest x2 4.33 us: modulate(): return (normed * (1.0 + rows[2 + row_index]) + rows[row_index]).astype(bf16)]
    pallas_call x3 -> x1, Pallas kernels: 78 us -> 74.1 us  [body(): pl.pallas_call(functools.partial(mixer_kernel, sp, tp, heads, per), in_sp...]
    unnamed x21 -> x1, local copies, waits for them, and re-layouts: 5.03 us -> 2.26 us
    another operation x2 -> x0, local copies, waits for them, and re-layouts: 1.37 us -> none  [body(): stacked = jnp.stack([condition, context_condition]).astype(f32)]
    dynamic_slice x2 -> x0, local copies, waits for them, and re-layouts: 1.12 us -> none  [own_heads(): lax.dynamic_slice_in_dim(array, first_head, heads_here, array.ndim - 1)]
where the time goes in v1:
time: 76.6 us; the launch traced here: 76.4 us
  Pallas kernels  74.1 us (97%)
  local copies, waits for them, and re-layouts  2.26 us (3%)
    pallas_call x1, Pallas kernels, body(): pl.pallas_call(functools.partial(mixer_kernel, sp, tp, heads, per), in_sp...  74.1 us
    unnamed x1, local copies, waits for them, and re-layouts  2.26 us

profile of v1, /device:TPU:0, one launch (start us, length us, event | category | flops | bytes accessed | tf_op | source)
XLA Modules:
  0.0 76.4 jit_solution(1152567963258363062)
XLA Ops:
  0.0 74.1 %mixer.1 = bf16[512,1024]{1,0:T(8,128)(2,1)} custom-call(bf16[4,128]{1,0:T(4,128)(2,1)} %bitcast.13, bf16[4,128]{1,0:T(4,128)(2,1)} %bitcast.14, f32[1,4096]{1,0:T(1,128)} %bitcast.12, f32[1,128]{1,0:T(1,128)} %bitcast.15, f32[2,16]{1,0:T(2,128)} %wb_ref.1, f32[2,16]{1,0:T(2,128)} %db_ref.1, f32[2,16]{1,0:T(2,128)} %lr_ref.1, bf16[512,1024]{1,0:T(8,128)(2,1)} %shift_ref.1, ...), custom_call_target="tpu_custom_call" | custom-call | tf_op jit(solution)/shard_map/mixer/pallas_call | solution.py:801
  74.1 2.3 %copy.20 = bf16[512,1024]{1,0:T(8,128)(2,1)} copy(bf16[512,1024]{1,0:T(8,128)(2,1)} %mixer.1) | data formatting | bytes 2097152

commit v2 on v1

--- a/solution.py
+++ b/solution.py
@@ -46,22 +46,84 @@
     )
 
 
-def start_inverse(item, rows, cols):
-    near = (rows // 2) == (cols // 2)
-    item["inv"] = jnp.where(rows == cols, 1.0, jnp.where(near, -item["system"], 0.0))
-
-
-def finish_inverse(items, size):
-    span = 2
-    while span < size:
+def bits(mask):
+    return mask.astype(f32).astype(bf16)
+
+
+def half_masks(size):
+    half = size // 2
+    lanes = lax.broadcasted_iota(jnp.int32, (half, size), 1)
+    return bits(lanes < half), bits(lanes >= half)
+
+
+def spread(compact, masks):
+    return jnp.concatenate([compact * masks[0], compact * masks[1]], axis=0)
+
+
+def invert_halves(items):
+    for item in items:
+        size = item["system"].shape[0]
+        half = size // 2
+        item["masks"] = half_masks(size)
+        item["system"] = item["system"].astype(bf16)
+        item["pieces"] = item["system"][:half] * item["masks"][0] + item["system"][half:] * item["masks"][1]
+        rows = lax.broadcasted_iota(jnp.int32, (half, size), 0)
+        cols = lax.rem(lax.broadcasted_iota(jnp.int32, (half, size), 1), half)
+        item["grid"] = (rows, cols)
+        item["inv"] = bits(rows == cols) - item["pieces"] * bits((rows // 2) == (cols // 2))
+    step = 2
+    while step < max(item["inv"].shape[0] for item in items):
         firsts = []
-        for item in items:
-            late, early = item["late_axis"] // span, item["early_axis"] // span
-            mask = ((late % 2) == 1) & (early == late - 1)
-            firsts.append(mm(jnp.where(mask, item["system"], 0.0), item["inv"]))
-        for item, first in zip(items, firsts):
-            item["inv"] = item["inv"] - mm(item["inv"], first)
-        span *= 2
+        active = [item for item in items if step < item["inv"].shape[0]]
+        for item in active:
+            rows, cols = item["grid"]
+            late, early = item["order"](rows, cols)
+            late, early = late // step, early // step
+            mask = bits(((late % 2) == 1) & (early == late - 1))
+            firsts.append(mm(item["pieces"] * mask, spread(item["inv"], item["masks"])).astype(bf16))
+        for item, first in zip(active, firsts):
+            item["inv"] = item["inv"] - mm(item["inv"], spread(first, item["masks"])).astype(bf16)
+        step *= 2
+
+
+def solve_halves(items):
+    def halves(item):
+        half = item["inv"].shape[0]
+        first, second = item["masks"]
+        return half, first, second
+
+    for item in items:
+        half, first, second = halves(item)
+        both = item["both"].astype(bf16)
+        lead = item["pick"](first, second)
+        item["lead"] = mm(item["inv"] * lead, both).astype(bf16)
+    for item in items:
+        half, first, second = halves(item)
+        lead = item["lead"]
+        mix = item["pick"](item["system"][half:] * first, item["system"][:half] * second)
+        item["rest"] = item["pick"](item["both"][half:], item["both"][:half]) - mm(
+            mix, jnp.concatenate([lead, lead], axis=0)
+        )
+    for item in items:
+        half, first, second = halves(item)
+        rest = item["rest"].astype(bf16)
+        trail = mm(
+            item["inv"] * item["pick"](second, first), jnp.concatenate([rest, rest], axis=0)
+        ).astype(bf16)
+        lead = item["lead"]
+        item["solved"] = jnp.concatenate([item["pick"](lead, trail), item["pick"](trail, lead)], axis=0)
+
+
+def chooser(d):
+    if isinstance(d, int):
+        return lambda a, b: a if d == 0 else b
+    return lambda a, b: jnp.where(d == 0, a, b)
+
+
+def orderer(d):
+    if isinstance(d, int):
+        return lambda a, b: (a, b) if d == 0 else (b, a)
+    return lambda a, b: (jnp.where(d == 0, a, b), jnp.where(d == 0, b, a))
 
 
 def key_grams(keys):
@@ -80,50 +142,98 @@
     return (rows == cols).astype(f32)
 
 
-def prepare_maps(tokens, span, k_ref, v_ref, col_ref, row_ref, srow_ref, solved_ref, carry_ref, map_ref):
+def make_item(d, gram, keys, keys_t, values, rate_col, run_col, run_row):
+    rows, cols = grid_iota(gram.shape[0])
+    order = orderer(d)
+    late, early = order(rows, cols)
+    decay = jnp.where(late > early, jnp.exp(jnp.minimum(run_col - run_row, 0.0)), 0.0)
+    both = jnp.concatenate([values * rate_col, keys * (rate_col * jnp.exp(run_col))], axis=1)
+    size = gram.shape[0]
+    last = chooser(d)(run_row[:, size - 1 :], run_row[:, :1])
+    return dict(
+        order=order,
+        pick=chooser(d),
+        system=gram * decay * rate_col,
+        both=both,
+        gate=jnp.exp(last),
+        late_t=(keys_t * jnp.exp(last - run_row)).astype(bf16),
+    )
+
+
+def latent_items(tokens, span, refs):
     size = min(CHUNK, tokens)
-    rows, cols = grid_iota(size)
+    k_ref, v_ref, col_ref, row_ref, srow_ref = refs[:5]
     items = []
-    shared = []
     for at in range(0, tokens, size):
         gram, keys, keys_t, s_row = key_grams(k_ref[at : at + size, :])
         srow_ref[:, at : at + size] = s_row
-        shared.append((keys, keys_t, v_ref[at : at + size, :].astype(f32)))
+        values = v_ref[at : at + size, :].astype(f32)
         for d in range(2):
             rate_col = col_ref[at : at + size, span * d : span * d + 1]
             run_col = col_ref[at : at + size, span * (2 + d) : span * (2 + d) + 1]
             run_row = row_ref[2 + d : 3 + d, at : at + size]
-            strict = rows > cols if d == 0 else rows < cols
-            decay = jnp.where(strict, jnp.exp(jnp.minimum(run_col - run_row, 0.0)), 0.0)
-            item = dict(at=at, d=d, rate_col=rate_col, run_col=run_col, run_row=run_row)
-            item["system"] = gram * decay * rate_col
-            item["late_axis"], item["early_axis"] = (rows, cols) if d == 0 else (cols, rows)
-            start_inverse(item, rows, cols)
+            item = make_item(d, gram, keys, keys_t, values, rate_col, run_col, run_row)
+            item["d"], item["index"] = d, at // size
             items.append(item)
-    finish_inverse(items, size)
+    return items
+
+
+def context_items(places, d, k_ref, v_ref, g_ref):
+    size = k_ref.shape[1]
+    items = []
+    for step in range(places):
+        place = step + d * (places - 1 - 2 * step)
+        gram, keys, keys_t, unused = key_grams(k_ref[place])
+        gates = g_ref[place]
+        gates_t = gates.T
+        items.append(
+            make_item(
+                d, gram, keys, keys_t, v_ref[place].astype(f32),
+                gates_t[:size, 0:1], gates_t[:size, 1:2], gates[1:2, :size],
+            )
+        )
+    return items
+
+
+def solve_items(items):
+    invert_halves(items)
+    solve_halves(items)
     for item in items:
-        keys, keys_t, values = shared[item["at"] // size]
-        growth = jnp.exp(item["run_col"])
-        both = jnp.concatenate([values * item["rate_col"], keys * (item["rate_col"] * growth)], axis=1)
-        solved = mm(item["inv"], both).astype(bf16)
-        solved_ref[item["at"] // size, item["d"]] = solved
-        last = item["run_row"][:, size - 1 :] if item["d"] == 0 else item["run_row"][:, :1]
-        item["gate"] = jnp.exp(last)
-        item["late"] = mm(keys_t * jnp.exp(last - item["run_row"]), solved)
+        item["late"] = mm(item["late_t"], item["solved"])
+
+
+def latent_maps(groups):
     eye = eye_matrix()
-    for d in range(2):
-        chunks = [i for i in items if i["d"] == d]
-        carry = None
-        for item in chunks if d == 0 else chunks[::-1]:
+    chains = []
+    for items, refs in groups:
+        solved_ref, carry_ref, map_ref = refs[5:]
+        for item in items:
+            solved_ref[item["index"], item["d"]] = item["solved"]
+        for d in range(2):
+            chain = [i for i in items if i["d"] == d]
+            chains.append((chain if d == 0 else chain[::-1], d, carry_ref, map_ref))
+    carries = [None] * len(chains)
+    for position in range(len(chains[0][0])):
+        for which, (chain, d, carry_ref, map_ref) in enumerate(chains):
+            item = chain[position]
             late, gate = item["late"], item["gate"]
             fresh = jnp.concatenate([late[:, :HEAD_DIM], (gate - 1.0) * eye - late[:, HEAD_DIM:]], axis=1)
-            if carry is None:
-                carry = fresh
+            if position == 0:
+                carries[which] = fresh
             else:
-                held = carry.astype(bf16)
-                carry_ref[item["at"] // size, d] = held
-                carry = gate * carry + fresh - mm(late[:, HEAD_DIM:], held)
+                held = carries[which].astype(bf16)
+                carry_ref[item["index"], d] = held
+                carries[which] = gate * carries[which] + fresh - mm(late[:, HEAD_DIM:], held)
+    for carry, (chain, d, carry_ref, map_ref) in zip(carries, chains):
         map_ref[d] = carry.astype(bf16)
+
+
+def context_state(items):
+    state = items[0]["late"][:, :HEAD_DIM]
+    for item in items[1:]:
+        late = item["late"]
+        state = item["gate"] * state + late[:, :HEAD_DIM] - mm(late[:, HEAD_DIM:], state)
+    return state.astype(bf16)
 
 
 def prepare_outputs(tokens, span, q_ref, k_ref, col_ref, row_ref, srow_ref, solved_ref, carry_ref, o_ref, e_ref):
@@ -157,43 +267,6 @@
         o_ref[at : at + size, :] = total
 
 
-def context_state(places, d, k_ref, v_ref, g_ref):
-    size = k_ref.shape[1]
-    rows, cols = grid_iota(size)
-    items = []
-    for step in range(places):
-        place = step + d * (places - 1 - 2 * step)
-        gram, keys, keys_t, unused = key_grams(k_ref[place])
-        gates = g_ref[place]
-        gates_t = gates.T
-        rate_col, run_col, run_row = gates_t[:size, 0:1], gates_t[:size, 1:2], gates[1:2, :size]
-        item = dict(keys=keys, keys_t=keys_t, values=v_ref[place].astype(f32), rate_col=rate_col)
-        item["run_col"], item["run_row"] = run_col, run_row
-        item["late_axis"] = jnp.where(d == 0, rows, cols)
-        item["early_axis"] = jnp.where(d == 0, cols, rows)
-        strict = item["late_axis"] > item["early_axis"]
-        decay = jnp.where(strict, jnp.exp(jnp.minimum(run_col - run_row, 0.0)), 0.0)
-        item["system"] = gram * decay * rate_col
-        start_inverse(item, rows, cols)
-        items.append(item)
-    finish_inverse(items, size)
-    for item in items:
-        growth = jnp.exp(item["run_col"])
-        both = jnp.concatenate(
-            [item["values"] * item["rate_col"], item["keys"] * (item["rate_col"] * growth)], axis=1
-        )
-        solved = mm(item["inv"], both)
-        run_row = item["run_row"]
-        last = jnp.where(d == 0, run_row[:, size - 1 :], run_row[:, :1])
-        item["gate"] = jnp.exp(last)
-        item["late"] = mm(item["keys_t"] * jnp.exp(last - run_row), solved)
-    state = items[0]["late"][:, :HEAD_DIM]
-    for item in items[1:]:
-        late = item["late"]
-        state = item["gate"] * state + late[:, :HEAD_DIM] - mm(late[:, HEAD_DIM:], state)
-    return state
-
-
 def log1p_unit(u):
     z = u / (2.0 + u)
     z2 = z * z
@@ -299,24 +372,37 @@
     for r, device in enumerate(cross):
         out.append(send(blocks.at[col], blocks.at[col], sent_b.at[r], recv_b.at[col], device))
         out[-1].start()
-    for r in range(1, tp):
-        src = lax.rem(col + r, tp)
+    core = lax.rem(col, 2)
+    partner = col + 1 - 2 * core
+    chips = tp // 2
+    far = [lax.rem(col + 2 * r, tp) for r in range(1, chips)]
+    far_partner = [place + 1 - 2 * core for place in far]
+
+    def block_arrive(src):
         send(blocks.at[src], blocks.at[src], sent_b.at[0], recv_b.at[src], on_mesh(tp=src)).wait_recv()
 
-    def modulate_rows(start, count, index):
-        for place in range(tp):
-            lanes = slice(place * width, (place + 1) * width)
-            block = blocks[place]
-            slope = gain_ref[:, lanes] * (1.0 + block[2 + index : 3 + index])
-            shift = block[index : index + 1]
-
-            def modulate(i, unused):
-                at = pl.ds(pl.multiple_of(start + i * step, step), step)
-                scale = jnp.concatenate([rstd[at, :]] * (width // 128), axis=1)
-                mixed[at, lanes] = (rows_in[at, lanes].astype(f32) * scale * slope + shift).astype(bf16)
-                return unused
-
-            lax.fori_loop(0, count // step, modulate, 0)
+    def modulate_rows(place, start, count, index):
+        lanes = pl.ds(pl.multiple_of(place * width, width), width)
+        block = blocks[place]
+        slope = gain_ref[:, lanes] * (1.0 + block[2 + index : 3 + index])
+        shift = block[index : index + 1]
+
+        def modulate(i, unused):
+            at = pl.ds(pl.multiple_of(start + i * step, step), step)
+            scale = jnp.concatenate([rstd[at, :]] * (width // 128), axis=1)
+            mixed[at, lanes] = (rows_in[at, lanes].astype(f32) * scale * slope + shift).astype(bf16)
+            return unused
+
+        lax.fori_loop(0, count // step, modulate, 0)
+
+    modulate_rows(col, tokens, ctx_tokens, 1)
+    modulate_rows(col, 0, tokens, 0)
+    block_arrive(partner)
+    modulate_rows(partner, tokens, ctx_tokens, 1)
+    modulate_rows(partner, 0, tokens, 0)
+    for place in far + far_partner:
+        block_arrive(place)
+        modulate_rows(place, tokens, ctx_tokens, 1)
 
     tile = 256 if out_width % 256 == 0 else 128
 
@@ -358,7 +444,6 @@
 
     for proj in projs[:2]:
         proj.wait()
-    modulate_rows(tokens, ctx_tokens, 1)
     ctx_gates = make_gates(tokens, ctx_tokens, ctx_tokens)
     if ctx_tokens < 128:
         ctx_gates = jnp.concatenate([ctx_gates, jnp.zeros((128 - ctx_tokens, 128), f32)], axis=0)
@@ -405,9 +490,13 @@
             ctx_v[slot, me] = v_s[tokens : tokens + ctx_tokens, lanes]
             ctx_g[slot, me] = ctx_send[item]
 
-    modulate_rows(0, tokens, 0)
+    for place in far + far_partner:
+        modulate_rows(place, 0, tokens, 0)
     size = min(CHUNK, tokens)
     gates = make_gates(0, tokens, size)
+    for j in range(out_width // tile):
+        lanes = slice(j * tile, (j + 1) * tile)
+        k_s[0:tokens, lanes] = jnp.dot(mixed[0:tokens, :], weights[:, lanes], preferred_element_type=f32).astype(bf16)
     for at in range(0, tokens, 128):
         block_t = gates[at : at + 128].T
         for head in range(heads):
@@ -418,10 +507,7 @@
                 + [jnp.zeros((4, 128), f32)],
                 axis=0,
             )
-    project(0, tokens, 0, k_s, 0)
     project(0, tokens, 1, v_s, 0)
-    projs[4].wait()
-    project(0, tokens, 2, q_s, 0)
 
     blocks_here = sp // 2
     one_way = lax.rem(me + 1, 2)
@@ -439,46 +525,47 @@
     out_step = 1 - 2 * other_way
     in_step = 1 - 2 * one_way
 
-    def stage_a(head):
+    def refs_of(head):
         lanes = lanes_of(head)
-        prepare_maps(
-            tokens,
-            span,
-            k_s.at[:, lanes],
-            v_s.at[:, lanes],
-            cols.at[head],
-            rows_g.at[head],
-            srow.at[head],
-            solved.at[head],
-            carry.at[head],
-            maps.at[head],
+        return (
+            k_s.at[:, lanes], v_s.at[:, lanes], cols.at[head], rows_g.at[head], srow.at[head],
+            solved.at[head], carry.at[head], maps.at[head],
         )
-        map_copy(head, out_step).start()
-
-    def stage_b(head):
-        lanes = lanes_of(head)
-        prepare_outputs(
-            tokens,
-            span,
-            q_s.at[:, lanes],
-            k_s.at[:, lanes],
-            cols.at[head],
-            rows_g.at[head],
-            srow.at[head],
-            solved.at[head],
-            carry.at[head],
-            o_s.at[head],
-            e_s.at[head],
-        )
-
-    def stage_pair(head):
-        map_copy(head, -in_step).wait_recv()
-        theirs, mine = got_map[head], maps[head, one_way]
-        pair_map[head] = (
-            theirs.astype(f32)
-            + mine.astype(f32)
-            + jnp.dot(mine[:, HEAD_DIM:], theirs, preferred_element_type=f32)
-        )
+
+    def stage_a(members, extra=()):
+        groups = [(latent_items(tokens, span, refs_of(head)), refs_of(head)) for head in members]
+        solve_items([item for group, unused in groups for item in group] + list(extra))
+        latent_maps(groups)
+        for head in members:
+            map_copy(head, out_step).start()
+
+    def stage_b(members):
+        for head in members:
+            lanes = lanes_of(head)
+            prepare_outputs(
+                tokens,
+                span,
+                q_s.at[:, lanes],
+                k_s.at[:, lanes],
+                cols.at[head],
+                rows_g.at[head],
+                srow.at[head],
+                solved.at[head],
+                carry.at[head],
+                o_s.at[head],
+                e_s.at[head],
+            )
+
+    def stage_pair(members):
+        for head in members:
+            map_copy(head, -in_step).wait_recv()
+        for head in members:
+            theirs, mine = got_map[head], maps[head, one_way]
+            pair_map[head] = (
+                theirs.astype(f32)
+                + mine.astype(f32)
+                + jnp.dot(mine[:, HEAD_DIM:], theirs, preferred_element_type=f32)
+            )
 
     def first_devices(d):
         return [d * (sp - 1) + (1 - 2 * d) * i for i in range(2)]
@@ -493,28 +580,27 @@
             on_mesh(sp=first_devices(d)[j]),
         )
 
-    def stage_context():
-        for slot in range(per):
-            item = me * per + slot
-
-            @pl.when(item < items)
+    def context_wait(slot):
+        for r in range(1, sp):
+            src = lax.rem(me + r, sp)
+            for j, spot in enumerate((ctx_k.at[slot, src], ctx_v.at[slot, src], ctx_g.at[slot, src])):
+                send(spot, spot, sent_c.at[0, j], recv_c.at[slot, src, j], on_mesh(sp=src)).wait_recv()
+
+    def context_parts(slot, item):
+        return context_items(sp, lax.rem(item, 2), ctx_k.at[slot], ctx_v.at[slot], ctx_g.at[slot])
+
+    def context_ship(slot, item, state):
+        s_zero[slot] = state
+        for j in range(2):
+            device, copy = zero_copy(slot, item, j)
+
+            @pl.when(device != me)
             def _():
-                for r in range(1, sp):
-                    src = lax.rem(me + r, sp)
-                    for j, spot in enumerate((ctx_k.at[slot, src], ctx_v.at[slot, src], ctx_g.at[slot, src])):
-                        send(spot, spot, sent_c.at[0, j], recv_c.at[slot, src, j], on_mesh(sp=src)).wait_recv()
-                state = context_state(sp, lax.rem(item, 2), ctx_k.at[slot], ctx_v.at[slot], ctx_g.at[slot])
-                s_zero[slot] = state.astype(bf16)
-                for j in range(2):
-                    device, copy = zero_copy(slot, item, j)
-
-                    @pl.when(device != me)
-                    def _():
-                        copy.start()
-
-                    @pl.when(device == me)
-                    def _():
-                        start_in[item // 2, lax.rem(item, 2)] = state.astype(bf16)
+                copy.start()
+
+            @pl.when(device == me)
+            def _():
+                start_in[item // 2, lax.rem(item, 2)] = state
 
     def rank_block(d):
         return (d * (sp - 1) + (1 - 2 * d) * me) // 2
@@ -529,46 +615,47 @@
             on_mesh(sp=me + in_step * (2 - j)),
         )
 
-    def stage_state(head, d):
+    def stage_state(members, d):
         block = rank_block(d)
-        owner = (2 * head + d) // per
-
-        @pl.when((block > 0) | (owner != me))
-        def _():
-            spot = start_in.at[head, d]
-            send(spot, spot, sent_h.at[head, 0], recv_s.at[head, d], on_mesh(sp=lax.rem(me + 1, sp))).wait_recv()
-
-        state = start_in[head, d]
-
-        @pl.when(d == one_way)
-        def _():
-            @pl.when(block < blocks_here - 1)
+        moving = (d == one_way) & (block < blocks_here - 1)
+        for head in members:
+            owner = (2 * head + d) // per
+
+            @pl.when((block > 0) | (owner != me))
             def _():
+                spot = start_in.at[head, d]
+                send(spot, spot, sent_h.at[head, 0], recv_s.at[head, d], on_mesh(sp=lax.rem(me + 1, sp))).wait_recv()
+
+            @pl.when(moving)
+            def _():
+                state = start_in[head, d]
                 pair = pair_map[head]
                 hop_out[head] = (
                     state.astype(f32)
                     + pair[:, :HEAD_DIM]
                     + jnp.dot(pair[:, HEAD_DIM:].astype(bf16), state, preferred_element_type=f32)
                 ).astype(bf16)
-                for j in range(2):
-                    hop_copy(head, j).start()
-
-            theirs = got_map[head]
-            start_own[head, d] = (
-                state.astype(f32)
-                + theirs[:, :HEAD_DIM].astype(f32)
-                + jnp.dot(theirs[:, HEAD_DIM:], state, preferred_element_type=f32)
-            ).astype(bf16)
+                hop_copy(head, 0).start()
+
+        @pl.when(moving)
+        def _():
+            for head in members:
+                hop_copy(head, 1).start()
+
+        @pl.when(d == one_way)
+        def _():
+            for head in members:
+                state, theirs = start_in[head, d], got_map[head]
+                start_own[head, d] = (
+                    state.astype(f32)
+                    + theirs[:, :HEAD_DIM].astype(f32)
+                    + jnp.dot(theirs[:, HEAD_DIM:], state, preferred_element_type=f32)
+                ).astype(bf16)
 
         @pl.when(d != one_way)
         def _():
-            start_own[head, d] = state
-
-    core = lax.rem(col, 2)
-    partner = col + 1 - 2 * core
-    chips = tp // 2
-    far = [lax.rem(col + 2 * r, tp) for r in range(1, chips)]
-    far_partner = [place + 1 - 2 * core for place in far]
+            for head in members:
+                start_own[head, d] = start_in[head, d]
 
     def far_copy(head, r):
         spot = ho.at[col, head]
@@ -595,99 +682,120 @@
     near_block = rank_block(first_dir)
     far_block = blocks_here - 1 - near_block
 
-    def lag(block):
-        return 1 + 2 * block + jnp.where(block >= 2, 1, 0)
-
-    def slot_events(s):
-        head1 = s - lag(near_block)
-
-        @pl.when((head1 >= 0) & (head1 < heads))
-        def _():
-            stage_state(head1, first_dir)
-
-        head2 = s - lag(far_block)
-
-        @pl.when((head2 >= 0) & (head2 < heads))
-        def _():
-            stage_state(head2, 1 - first_dir)
-            stage_final(head2)
-
-    def loop_a(head, unused):
-        stage_a(head)
-
-        @pl.when(head == 0)
-        def _():
-            stage_context()
-
-        @pl.when(head > 0)
-        def _():
-            stage_pair(head - 1)
-
-        slot_events(head)
-        return unused
-
-    lax.fori_loop(0, heads, loop_a, 0)
-
-    def loop_b(head, unused):
-        stage_b(head)
-
-        @pl.when(head == 0)
-        def _():
-            stage_pair(heads - 1)
-
-        slot_events(heads + head)
-        return unused
-
-    lax.fori_loop(0, heads, loop_b, 0)
-    last_slot = heads + 1 + 2 * (blocks_here - 1) + (1 if blocks_here > 2 else 0)
-
-    def loop_c(s, unused):
-        slot_events(s)
-        return unused
-
-    lax.fori_loop(2 * heads, last_slot, loop_c, 0)
+    def near_event(members):
+        stage_state(members, first_dir)
+
+    def far_event(members):
+        stage_state(members, 1 - first_dir)
+        for head in members:
+            stage_final(head)
+
+    team = 2 if heads % 2 == 0 else 1
+    teams = [list(range(at, at + team)) for at in range(0, heads, team)]
+    for index, members in enumerate(teams):
+        if index == 0 and items == per * sp:
+            for slot in range(per):
+                context_wait(slot)
+            extras = [context_parts(slot, me * per + slot) for slot in range(per)]
+            stage_a(members, [item for extra in extras for item in extra])
+            for slot, extra in enumerate(extras):
+                context_ship(slot, me * per + slot, context_state(extra))
+        elif index == 0:
+            stage_a(members)
+            for slot in range(per):
+                item = me * per + slot
+
+                @pl.when(item < items)
+                def _():
+                    context_wait(slot)
+                    extra = context_parts(slot, item)
+                    solve_items(extra)
+                    context_ship(slot, item, context_state(extra))
+        else:
+            stage_a(members)
+            stage_pair(teams[index - 1])
+
+            @pl.when(near_block == 0)
+            def _():
+                near_event(teams[index - 1])
+
+    projs[4].wait()
+    project(0, tokens, 2, q_s, 0)
+    stage_pair(teams[-1])
+
+    @pl.when(near_block == 0)
+    def _():
+        near_event(teams[-1])
+
+    @pl.when(near_block > 0)
+    def _():
+        near_event(teams[0])
+
+    for members in teams:
+        stage_b(members)
+
+    @pl.when(near_block > 0)
+    def _():
+        for members in teams[1:]:
+            near_event(members)
+
+    for members in teams:
+        far_event(members)
     out_load.wait()
-    group = min(2, heads)
-
-    def add(src, first, count, start):
-        block = jnp.concatenate([ho[src, first + i] for i in range(count)], axis=1)
-
+    def multiply(spans, finish):
         def columns(j, unused):
             lanes = pl.ds(pl.multiple_of(j * tile, tile), tile)
-            at = pl.ds(pl.multiple_of(src * out_width + first * HEAD_DIM, HEAD_DIM), count * HEAD_DIM)
-            part = jnp.dot(block, wo[at, lanes], preferred_element_type=f32)
-            acc[:, lanes] = part if start else acc[:, lanes] + part
+            part = None
+            for src, first, count in spans:
+                block = jnp.concatenate([ho[src, first + i] for i in range(count)], axis=1)
+                at = pl.ds(pl.multiple_of(src * out_width + first * HEAD_DIM, HEAD_DIM), count * HEAD_DIM)
+                term = jnp.dot(block, wo[at, lanes], preferred_element_type=f32)
+                part = term if part is None else part + term
+            finish(j, lanes, part)
             return unused
 
         lax.fori_loop(0, width // tile, columns, 0)
 
-    add(col, 0, heads, True)
+    def first_part(j, lanes, part):
+        acc[:, lanes] = part
+
+    def middle_part(j, lanes, part):
+        acc[:, lanes] = acc[:, lanes] + part
+
+    def last_part(j, lanes, part):
+        residual = rows_in[pl.ds(0, tokens), pl.ds(pl.multiple_of(col * width + j * tile, tile), tile)].astype(f32)
+        out_ref[:, lanes] = (residual + gate_row[:, lanes] * (acc[:, lanes] + part)).astype(bf16)
+
     for head in range(heads):
         spot = ho.at[partner, head]
         send(spot, spot, sent_p.at[head], recv_p.at[head], on_mesh(tp=partner)).wait_recv()
-    add(partner, 0, heads, False)
-    for first in range(0, heads, group):
-        for head in range(first, first + group):
-            for r, src in enumerate(far):
-                spot = ho.at[src, head]
-                send(spot, spot, sent_y.at[head, r], recv_y.at[head, src], on_mesh(tp=src)).wait_recv()
-                relay_copy(head, r).start()
-        for src in far:
-            add(src, first, group, False)
-        for head in range(first, first + group):
-            for r, src in enumerate(far_partner):
-                spot = ho.at[src, head]
-                send(spot, spot, sent_r.at[head, r], recv_r.at[head, src], on_mesh(tp=partner)).wait_recv()
-        for src in far_partner:
-            add(src, first, group, False)
-
-    def finish(i, unused):
-        at = pl.ds(pl.multiple_of(i * step, step), step)
-        residual = rows_in[at, pl.ds(pl.multiple_of(col * width, width), width)].astype(f32)
-        out_ref[at, :] = (residual + gate_row[...] * acc[at, :]).astype(bf16)
-        return unused
-
-    lax.fori_loop(0, tokens // step, finish, 0)
+    multiply([(col, 0, heads), (partner, 0, heads)], first_part)
+    def far_arrive(head):
+        for r, src in enumerate(far):
+            spot = ho.at[src, head]
+            send(spot, spot, sent_y.at[head, r], recv_y.at[head, src], on_mesh(tp=src)).wait_recv()
+            relay_copy(head, r).start()
+
+    def relay_arrive(head):
+        for r, src in enumerate(far_partner):
+            spot = ho.at[src, head]
+            send(spot, spot, sent_r.at[head, r], recv_r.at[head, src], on_mesh(tp=partner)).wait_recv()
+
+    for members in teams[:-1]:
+        for head in members:
+            far_arrive(head)
+        for head in members:
+            relay_arrive(head)
+        multiply([(src, members[0], len(members)) for src in far + far_partner], middle_part)
+    for head in teams[-1]:
+        far_arrive(head)
+        if head < heads - 1:
+            relay_arrive(head)
+            multiply([(src, head, 1) for src in far + far_partner], middle_part)
+        else:
+            multiply([(src, head, 1) for src in far], middle_part)
+            relay_arrive(head)
+            multiply([(src, head, 1) for src in far_partner], last_part)
     for copy in out:
         copy.wait_send()
     for item in range(items):

time: 76.6 us -> 69.6 us (0.909)
  Pallas kernels: 74.1 us -> 67.1 us
    pallas_call x1, Pallas kernels: 74.1 us -> 67.1 us  [body(): pl.pallas_call(functools.partial(mixer_kernel, sp, tp, heads, per), in_sp...]
where the time goes in v2:
time: 69.6 us; the launch traced here: 69.4 us
  Pallas kernels  67.1 us (96%)
  local copies, waits for them, and re-layouts  2.26 us (3%)
    pallas_call x1, Pallas kernels, body(): pl.pallas_call(functools.partial(mixer_kernel, sp, tp, heads, per), in_sp...  67.1 us
    unnamed x1, local copies, waits for them, and re-layouts  2.26 us

profile of v2, /device:TPU:0, one launch (start us, length us, event | category | flops | bytes accessed | tf_op | source)
XLA Modules:
  0.0 69.4 jit_solution(4477025038115982400)
XLA Ops:
  0.0 67.1 %mixer.1 = bf16[512,1024]{1,0:T(8,128)(2,1)} custom-call(bf16[4,128]{1,0:T(4,128)(2,1)} %bitcast.13, bf16[4,128]{1,0:T(4,128)(2,1)} %bitcast.14, f32[1,4096]{1,0:T(1,128)} %bitcast.12, f32[1,128]{1,0:T(1,128)} %bitcast.15, f32[2,16]{1,0:T(2,128)} %wb_ref.1, f32[2,16]{1,0:T(2,128)} %db_ref.1, f32[2,16]{1,0:T(2,128)} %lr_ref.1, bf16[512,1024]{1,0:T(8,128)(2,1)} %shift_ref.1, ...), custom_call_target="tpu_custom_call" | custom-call | tf_op jit(solution)/shard_map/mixer/pallas_call | solution.py:909
  67.1 2.3 %copy.20 = bf16[512,1024]{1,0:T(8,128)(2,1)} copy(bf16[512,1024]{1,0:T(8,128)(2,1)} %mixer.1) | data formatting | bytes 2097152

commit v3 on v2

--- a/solution.py
+++ b/solution.py
@@ -683,11 +683,12 @@
     far_block = blocks_here - 1 - near_block
 
     def near_event(members):
-        stage_state(members, first_dir)
+        for head in members:
+            stage_state([head], first_dir)
 
     def far_event(members):
-        stage_state(members, 1 - first_dir)
         for head in members:
+            stage_state([head], 1 - first_dir)
             stage_final(head)
 
     team = 2 if heads % 2 == 0 else 1
@@ -713,19 +714,21 @@
                     context_ship(slot, item, context_state(extra))
         else:
             stage_a(members)
-            stage_pair(teams[index - 1])
-
-            @pl.when(near_block == 0)
-            def _():
-                near_event(teams[index - 1])
+            for head in teams[index - 1]:
+                stage_pair([head])
+
+                @pl.when(near_block == 0)
+                def _():
+                    near_event([head])
 
     projs[4].wait()
     project(0, tokens, 2, q_s, 0)
-    stage_pair(teams[-1])
-
-    @pl.when(near_block == 0)
-    def _():
-        near_event(teams[-1])
+    for head in teams[-1]:
+        stage_pair([head])
+
+        @pl.when(near_block == 0)
+        def _():
+            near_event([head])
 
     @pl.when(near_block > 0)
     def _():

time: 69.6 us -> 69.1 us (level)
  no operation moved by 1% of the time
where the time goes in v3:
time: 69.1 us; the launch traced here: 68.8 us
  Pallas kernels  66.5 us (96%)
  local copies, waits for them, and re-layouts  2.26 us (3%)
    pallas_call x1, Pallas kernels, body(): pl.pallas_call(functools.partial(mixer_kernel, sp, tp, heads, per), in_sp...  66.5 us
    unnamed x1, local copies, waits for them, and re-layouts  2.26 us

profile of v3, /device:TPU:0, one launch (start us, length us, event | category | flops | bytes accessed | tf_op | source)
XLA Modules:
  0.0 68.8 jit_solution(1963022024419411428)
XLA Ops:
  0.0 66.5 %mixer.1 = bf16[512,1024]{1,0:T(8,128)(2,1)} custom-call(bf16[4,128]{1,0:T(4,128)(2,1)} %bitcast.13, bf16[4,128]{1,0:T(4,128)(2,1)} %bitcast.14, f32[1,4096]{1,0:T(1,128)} %bitcast.12, f32[1,128]{1,0:T(1,128)} %bitcast.15, f32[2,16]{1,0:T(2,128)} %wb_ref.1, f32[2,16]{1,0:T(2,128)} %db_ref.1, f32[2,16]{1,0:T(2,128)} %lr_ref.1, bf16[512,1024]{1,0:T(8,128)(2,1)} %shift_ref.1, ...), custom_call_target="tpu_custom_call" | custom-call | tf_op jit(solution)/shard_map/mixer/pallas_call | solution.py:912
  66.5 2.3 %copy.20 = bf16[512,1024]{1,0:T(8,128)(2,1)} copy(bf16[512,1024]{1,0:T(8,128)(2,1)} %mixer.1) | data formatting | bytes 2097152
